TPU v7x, 512 devices: a whole 4x4x16 slice. The times are simulated.
512 devices in a mesh: row: 32 (over z, core), col: 16 (over y, x).
Axes of the slice: x: 4, y: 4, z: 16, core: 2. Of those that a mesh axis runs over, the one named last changes fastest.
Arguments:
- tokens: bfloat16 [1, 8192, 2048], P(None, 'row'), may hold values from -6 to 6
- w_value: bfloat16 [2048, 1024], P(None, 'col'), may hold values from -0.125 to 0.125
- w_first: bfloat16 [2048, 1024], P(None, 'col'), may hold values from -0.125 to 0.125
- w_second: bfloat16 [2048, 1024], P(None, 'col'), may hold values from -0.125 to 0.125
- w_gate: bfloat16 [2048, 1024], P(None, 'col'), may hold values from -0.125 to 0.125
- conv_taps: float32 [3, 3, 1024], P(None, None, 'col'), may hold values from -3.5 to 3.5
- filter_embed: float32 [33, 64], replicated, may hold values from -192 to 192
- filter_freq: float32 [64], replicated, may hold values from 0.1 to 1.9
- filter_proj: float32 [64, 2, 2, 1024], P(None, None, None, 'col'), may hold values from -0.01171875 to 0.01171875
- filter_decay: float32 [2, 2, 1024], P(None, None, 'col'), may hold values from 0.25 to 128
- skip_gain: float32 [2, 1024], P(None, 'col'), may hold values from -3 to 3
- w_out: bfloat16 [1024, 2048], P('col'), may hold values from -0.1875 to 0.1875
Outputs:
- mixed: bfloat16 [1, 8192, 2048], P(None, ('row', 'col'))
All inputs are finite; a program needn't handle non-finite values.
Results may differ from a plain program's by a relative error of at most 0.018.
Values may be sent and summed in bfloat16 or wider, within the bound.
A program may use at most 64 MiB of HBM per device.

v0:
```python
import functools
import math

import jax
import jax.numpy as jnp
import ml_dtypes
import numpy as np
from jax import lax
from jax.experimental import pallas as pl
from jax.experimental.pallas import tpu as pltpu
from jax.sharding import PartitionSpec as P

MESH = pl.DeviceIdType.MESH
F32 = jnp.float32
BF16 = jnp.bfloat16

LENGTH = 8192
ROWS = 32
COLS = 16
FEATS = 33
FEAT_STEP = 40


def halves(x):
    x = np.asarray(x, np.float64)
    high = x.astype(ml_dtypes.bfloat16)
    low = (x - high.astype(np.float64)).astype(ml_dtypes.bfloat16)
    return high, low


@functools.lru_cache(None)
def constants():
    two_pi = 2.0 * math.pi
    j = np.arange(64)
    q = 2 * (j % 32) + j // 32
    k1 = np.arange(64) + 0.5
    p = np.arange(128)
    first = np.concatenate([np.cos(two_pi * np.outer(k1, q) / 128), -np.sin(two_pi * np.outer(k1, q) / 128)], axis=0)
    f_high, f_low = halves(first)
    outer_in = np.concatenate([f_high, f_high, f_low], axis=1)
    outer_out = np.concatenate([f_high.T, f_high.T, f_low.T], axis=1)
    twist = np.stack(
        [np.cos(two_pi * np.outer(k1, p) / 16384), -np.sin(two_pi * np.outer(k1, p) / 16384)]
    ).astype(np.float32)
    g_real = np.cos(two_pi * (np.outer(p, p) % 128) / 128)
    g_imag = -np.sin(two_pi * (np.outer(p, p) % 128) / 128)
    inner_in = np.stack(halves(np.block([[g_real, g_imag], [-g_imag, g_real]])))
    inner_out = np.stack(halves(np.block([[g_real, -g_imag], [g_imag, g_real]])))
    n = np.arange(LENGTH)
    b = np.arange(1, 17)
    phase = two_pi * (np.outer(b, n) % LENGTH) / LENGTH
    features = np.concatenate([(n / (LENGTH - 1))[None], np.cos(phase), np.sin(phase)], axis=0)
    table = np.zeros((128, LENGTH), ml_dtypes.bfloat16)
    rest = features
    for part in range(3):
        piece = rest.astype(ml_dtypes.bfloat16)
        table[part * FEAT_STEP : part * FEAT_STEP + FEATS] = piece
        rest = rest - piece.astype(np.float64)
    return outer_in, outer_out, twist, inner_in, inner_out, table


def split(x):
    high = x.astype(BF16)
    return high, (x - high.astype(F32)).astype(BF16)


def dot(a, b):
    return jnp.dot(a, b, preferred_element_type=F32)


def dot_nt(a, b, precision=None):
    return lax.dot_general(a, b, (((1,), (1,)), ((), ())), precision=precision, preferred_element_type=F32)


def times(x, matrix):
    high, low = split(x)
    return dot(high, matrix[0]) + dot(low, matrix[0]) + dot(high, matrix[1])


def forward(signal, outer_in, twist, inner_in):
    high, low = split(signal)
    stage = dot(outer_in, jnp.concatenate([high, low, high], axis=0))
    turned = []
    for m in range(signal.shape[1] // 128):
        real = stage[:64, 128 * m : 128 * (m + 1)]
        imag = stage[64:, 128 * m : 128 * (m + 1)]
        turned.append(
            jnp.concatenate([real * twist[0] - imag * twist[1], real * twist[1] + imag * twist[0]], axis=1)
        )
    return times(jnp.concatenate(turned, axis=0), inner_in)


def inverse(spectrum, outer_out, twist, inner_out):
    stage = times(spectrum, inner_out)
    reals, imags = [], []
    for m in range(spectrum.shape[0] // 64):
        real = stage[64 * m : 64 * (m + 1), :128]
        imag = stage[64 * m : 64 * (m + 1), 128:]
        reals.append(real * twist[0] + imag * twist[1])
        imags.append(imag * twist[0] - real * twist[1])
    both = jnp.concatenate([jnp.concatenate(reals, axis=1), jnp.concatenate(imags, axis=1)], axis=0)
    high, low = split(both)
    return dot(outer_out, jnp.concatenate([high, low, high], axis=0))


def convolve(signal, filt, tables):
    outer_in, outer_out, twist, inner_in, inner_out = tables
    spectrum = forward(signal, outer_in, twist, inner_in)
    real, imag = spectrum[:, :128], spectrum[:, 128:]
    f_real, f_imag = filt[:, :128], filt[:, 128:]
    product = jnp.concatenate([real * f_real - imag * f_imag, real * f_imag + imag * f_real], axis=1)
    return inverse(product, outer_out, twist, inner_out)


def filter_spectrum(signals, outer_in, twist, inner_in):
    spectra = forward(signals, outer_in, twist, inner_in)
    ahead, behind = spectra[:128], spectra[128:]
    scale = 2.0 / (2 * LENGTH)
    return jnp.concatenate(
        [(ahead[:, :128] + behind[:, :128]) * scale, (ahead[:, 128:] - behind[:, 128:]) * scale], axis=1
    )


def sine(x):
    k = jnp.floor(x * (1.0 / math.pi) + 0.5)
    r = x - k * 3.140625
    r = r - k * 9.67502593994140625e-4
    r = r - k * 1.509957990978376432e-7
    half = k * 0.5
    sign = 1.0 - 4.0 * (half - jnp.floor(half))
    s = r * r
    poly = -1.0 / 39916800.0
    for c in (1.0 / 362880.0, -1.0 / 5040.0, 1.0 / 120.0, -1.0 / 6.0):
        poly = poly * s + c
    return sign * (r + r * (s * poly))


def shifted(parts, lane, sub):
    right = [pltpu.roll(x, 1, 1) for x in parts]
    left = [pltpu.roll(x, 127, 1) for x in parts]
    carry = jnp.where(sub == 0, 0.0, pltpu.roll(right[1], 1, 0))
    back = jnp.where(sub == 31, 0.0, pltpu.roll(left[0], 31, 0))
    before = [jnp.where(lane == 0, carry, right[0]), jnp.where(lane == 0, right[0], right[1])]
    after = [jnp.where(lane == 127, left[1], left[0]), jnp.where(lane == 127, back, left[1])]
    return before, after


def kernel(
    tokens, w_value, w_first, w_second, w_gate, conv_taps, embed, freq, proj, decay, gain, w_out,
    outer_in_h, outer_out_h, twist_h, inner_in_h, inner_out_h, table_h,
    out_ref,
    tok_v, w_v, taps_v, embed_v, freq_v, proj_v, decay_v, gain_v,
    outer_in_v, outer_out_v, twist_v, inner_in_v, inner_out_v, table_v,
    w_full, est, lag_taps, spectra, grid_v, send1, recv1, send2, recv2, back_v, send3, recv3, block_v, send4, recv4,
    load_sem, send_sem1, recv_sem1, send_sem2, recv_sem2, send_sem3, recv_sem3, send_sem4, recv_sem4,
    send_sem5, recv_sem5, swap_send, swap_recv,
):
    row = lax.axis_index("row")
    col = lax.axis_index("col")
    z = lax.div(row, 2)
    core = lax.rem(row, 2)
    partner = z * 2 + 1 - core

    def row_peers(visit):
        def step(i, carry):
            away = 8 + lax.div(i + 1, 2) * (1 - 2 * lax.rem(i, 2))
            there = lax.rem(z + away, 16) * 2
            visit(there)
            visit(there + 1)
            return carry

        lax.fori_loop(0, 15, step, 0)
        visit(partner)

    def col_peers(visit):
        def step(i, carry):
            visit(lax.rem(col + i, COLS))
            return carry

        lax.fori_loop(1, COLS, step, 0)

    barrier = pltpu.get_barrier_semaphore()
    row_peers(lambda r: pl.semaphore_signal(barrier, inc=1, device_id=(r, col), device_id_type=MESH))
    col_peers(lambda c: pl.semaphore_signal(barrier, inc=1, device_id=(row, c), device_id_type=MESH))

    own_rows = pl.ds(pl.multiple_of(col * 64, 64), 64)
    loads = []
    for source, target in (
        (tokens.at[0], tok_v),
        (w_value, w_v.at[0]),
        (w_first, w_v.at[1]),
        (w_second, w_v.at[2]),
        (w_gate, w_v.at[3]),
        (w_out.at[:, pl.ds(pl.multiple_of(core * 1024, 1024), 1024)], w_full.at[core, own_rows]),
        (conv_taps, taps_v),
        (embed, embed_v),
        (freq, freq_v),
        (proj, proj_v),
        (decay, decay_v),
        (gain, gain_v),
        (table_h, table_v),
        (outer_in_h, outer_in_v),
        (outer_out_h, outer_out_v),
        (twist_h, twist_v),
        (inner_in_h, inner_in_v),
        (inner_out_h, inner_out_v),
    ):
        load = pltpu.make_async_copy(source, target, load_sem.at[len(loads)])
        load.start()
        loads.append(load)

    for load in loads[:5]:
        load.wait()
    order = lax.broadcasted_iota(jnp.int32, (256, 64), 0)
    channel = lax.broadcasted_iota(jnp.int32, (256, 64), 1)
    own_channel = channel == 2 * (order >> 3) + ((order >> 1) & 1)
    place = [
        jnp.where(own_channel & ((order & 1) == h) & (((order >> 2) & 1) == k), 1.0, 0.0).astype(BF16)
        for k in range(2)
        for h in range(2)
    ]
    for pair, target in ((0, send1), (2, send2)):
        total = jnp.zeros((256, 128), F32)
        for k in range(2):
            result = dot(tok_v[...], w_v[pair + k]).astype(BF16)
            for h in range(2):
                total = total + dot_nt(place[2 * k + h], result[128 * h : 128 * (h + 1)])
        target[...] = total.reshape(ROWS, 8, 128).astype(BF16)
    recv1[pl.ds(row, 1)] = send1[pl.ds(row, 1)]
    recv2[pl.ds(row, 1)] = send2[pl.ds(row, 1)]
    loads[5].wait()

    def to_row(source, target, sent, received, r):
        return pltpu.make_async_remote_copy(
            src_ref=source.at[r], dst_ref=target.at[row], send_sem=sent.at[r], recv_sem=received.at[row],
            device_id=(r, col), device_id_type=MESH,
        )

    def from_row(source, target, sent, received, r):
        return pltpu.make_async_remote_copy(
            src_ref=source.at[r], dst_ref=target.at[r], send_sem=sent.at[r], recv_sem=received.at[r],
            device_id=(r, col), device_id_type=MESH,
        )

    def to_col(source, target, sent, received, c):
        return pltpu.make_async_remote_copy(
            src_ref=source.at[c], dst_ref=target.at[col], send_sem=sent.at[c], recv_sem=received.at[col],
            device_id=(row, c), device_id_type=MESH,
        )

    def from_col(source, target, sent, received, c):
        return pltpu.make_async_remote_copy(
            src_ref=source.at[c], dst_ref=target.at[c], send_sem=sent.at[c], recv_sem=received.at[c],
            device_id=(row, c), device_id_type=MESH,
        )

    def weight_rows(c):
        return w_full.at[core, pl.ds(pl.multiple_of(c * 64, 64), 64)]

    def weights_to(c):
        return pltpu.make_async_remote_copy(
            src_ref=weight_rows(col), dst_ref=weight_rows(col), send_sem=send_sem5.at[c], recv_sem=recv_sem5.at[col],
            device_id=(row, c), device_id_type=MESH,
        )

    def weights_from(c):
        return pltpu.make_async_remote_copy(
            src_ref=weight_rows(c), dst_ref=weight_rows(c), send_sem=send_sem5.at[c], recv_sem=recv_sem5.at[c],
            device_id=(row, c), device_id_type=MESH,
        )

    first_trip = (send1, recv1, send_sem1, recv_sem1)
    second_trip = (send2, recv2, send_sem2, recv_sem2)
    back_trip = (send3, recv3, send_sem3, recv_sem3)
    last_trip = (send4, recv4, send_sem4, recv_sem4)

    pl.semaphore_wait(barrier, ROWS - 1 + COLS - 1)
    row_peers(lambda r: to_row(*first_trip, r).start())
    row_peers(lambda r: to_row(*second_trip, r).start())
    col_peers(lambda c: weights_to(c).start())

    for load in loads[6:]:
        load.wait()
    scaled = embed_v[...] * freq_v[...]
    est[...] = jnp.zeros_like(est)
    high = scaled.astype(BF16).astype(F32)
    rest = scaled - high
    mid = rest.astype(BF16).astype(F32)
    low = rest - mid
    for k, parts in enumerate(((high, high, high), (mid, mid), (low,))):
        for m, part in enumerate(parts):
            est[k, FEAT_STEP * m : FEAT_STEP * m + FEATS, :64] = part
    layer = jnp.concatenate([jnp.transpose(est[k])[:64] for k in range(3)], axis=0).astype(BF16)

    lane64 = lax.broadcasted_iota(jnp.int32, (8, 64), 1)
    sub64 = lax.broadcasted_iota(jnp.int32, (8, 64), 0)
    own_proj = jnp.zeros((8, 64), F32)
    for o in range(2):
        for d in range(2):
            pick = jnp.where((lane64 == 2 * row + (sub64 & 1)) & ((sub64 >> 1) == 2 * o + d), 1.0, 0.0)
            own_proj = own_proj + dot_nt(pick, proj_v[:, o, d, :], lax.Precision.HIGHEST)
    proj_high, proj_low = split(own_proj)
    proj_both = jnp.concatenate([own_proj, own_proj - proj_high.astype(F32)], axis=0).astype(BF16)

    def own(ref):
        lanes = lax.broadcasted_iota(jnp.int32, ref.shape, len(ref.shape) - 1)
        return [jnp.sum(jnp.where(lanes == 2 * row + c, ref[...], 0.0), axis=-1, keepdims=True) for c in range(2)]

    own_taps = own(taps_v)
    own_decay = own(decay_v)
    own_gain = own(gain_v)
    sub8 = lax.broadcasted_iota(jnp.int32, (8, 128), 0)
    decay_rows = jnp.zeros((8, 128), F32)
    start_rows = jnp.zeros((8, 128), F32)
    for o in range(2):
        for c in range(2):
            start_rows = jnp.where(sub8 == 4 * o + c, own_gain[c][o : o + 1], start_rows)
            for d in range(2):
                decay_rows = jnp.where(sub8 == 4 * o + 2 * d + c, own_decay[c][o, d : d + 1], decay_rows)
    lag8 = lax.broadcasted_iota(jnp.int32, (8, 128), 1)
    keep = ((sub8 >> 1) & 1) == 0

    def lags(step, carry):
        width = 1024
        block = table_v[:, pl.ds(pl.multiple_of(step * width, width), width)]
        parts = dot(layer, block)
        hidden = sine(parts[:64] + parts[64:128] + parts[128:])
        hid_high, hid_low = split(hidden)
        twice = dot(proj_both, hid_high)
        taps = twice[:8] + twice[8:] + dot(proj_high, hid_low)
        for i in range(width // 128):
            at = step * width + i * 128 + lag8
            piece = taps[:, 128 * i : 128 * (i + 1)] * jnp.exp(decay_rows * (at.astype(F32) * (-1.0 / (LENGTH - 1))))
            piece = jnp.where(at == 0, jnp.where(keep, piece + start_rows, 0.0), piece)
            to = ((i % 2) * 32 + i // 2 + step * 4) * 8
            lag_taps[pl.ds(pl.multiple_of(to, 8), 8), :] = piece
        return carry

    lax.fori_loop(0, LENGTH // 1024, lags, 0)

    twist = (twist_v[0], twist_v[1])
    inner_in = (inner_in_v[0], inner_in_v[1])
    inner_out = (inner_out_v[0], inner_out_v[1])
    for o in range(2):
        signals = jnp.concatenate([lag_taps[pl.ds(4 * o + k, 64, stride=8), :] for k in range(4)], axis=1)
        spectra[o] = filter_spectrum(signals, outer_in_v[...], twist, inner_in)
    tables = (outer_in_v[...], outer_out_v[...], twist, inner_in, inner_out)

    lane = lax.broadcasted_iota(jnp.int32, (32, 128), 1)
    sub = lax.broadcasted_iota(jnp.int32, (32, 128), 0)

    def arrived(buffer):
        grid_v[...] = buffer[...].astype(F32).reshape(ROWS * 8, 128)

    def loaded(k, c):
        return [grid_v[pl.ds(4 * k + 2 * c + h, 32, stride=8), :] for h in range(2)]

    def short(k, role):
        whole = []
        for c in range(2):
            here = loaded(k, c)
            before, after = shifted(here, lane, sub)
            weight = [own_taps[c][j, role : role + 1] for j in range(3)]
            whole.append(
                jnp.concatenate(
                    [before[h] * weight[0] + here[h] * weight[1] + after[h] * weight[2] for h in range(2)], axis=0
                )
            )
        return jnp.concatenate(whole, axis=1)

    row_peers(lambda r: from_row(*first_trip, r).wait_recv())
    arrived(recv1)
    value = short(0, 0)
    first = short(1, 1)
    inner = first * convolve(value, spectra[0], tables)
    second_conv = convolve(inner, spectra[1], tables)

    row_peers(lambda r: from_row(*second_trip, r).wait_recv())
    arrived(recv2)
    second = short(0, 2)
    gate = jnp.concatenate([jnp.concatenate(loaded(1, c), axis=0) for c in range(2)], axis=1)
    outer = second * second_conv * (gate / (1.0 + jnp.exp(-gate)))

    for c in range(2):
        for h in range(2):
            back_v[pl.ds(2 * c + h, 32, stride=8), :] = outer[32 * h : 32 * (h + 1), 128 * c : 128 * (c + 1)]
    for r in range(ROWS):
        send3[r] = back_v[8 * r : 8 * r + 4, :].astype(BF16)
    recv3[pl.ds(row, 1)] = send3[pl.ds(row, 1)]
    row_peers(lambda r: to_row(*back_trip, r).start())

    col_peers(lambda c: weights_from(c).wait_recv())
    swap = pltpu.make_async_remote_copy(
        src_ref=w_full.at[core], dst_ref=w_full.at[core], send_sem=swap_send, recv_sem=swap_recv,
        device_id=(partner, col), device_id_type=MESH,
    )
    swap.start()

    row_peers(lambda r: from_row(*back_trip, r).wait_recv())
    for r in range(ROWS):
        block_v[4 * r : 4 * r + 4, :] = recv3[r].astype(F32)
    flipped = jnp.transpose(block_v[...]).astype(BF16)
    i128 = lax.broadcasted_iota(jnp.int32, (128, 256), 0)
    l256 = lax.broadcasted_iota(jnp.int32, (128, 256), 1)
    spread = jnp.where(l256 == 128 * (i128 & 1) + 64 * lax.rem(col, 2) + (i128 >> 1), 1.0, 0.0).astype(BF16)
    rows = dot(flipped, spread).astype(BF16)
    for h in range(2):
        send4[8 * h : 8 * (h + 1)] = rows[:, 128 * h : 128 * (h + 1)].reshape(8, 16, 128)
    recv4[pl.ds(col, 1)] = send4[pl.ds(col, 1)]
    col_peers(lambda c: to_col(*last_trip, c).start())

    swap.wait()
    col_peers(lambda c: from_col(*last_trip, c).wait_recv())
    left = jnp.concatenate([recv4[2 * m] + recv4[2 * m + 1] for m in range(8)], axis=1)
    for k in range(2):
        out_ref[0, :, 1024 * k : 1024 * (k + 1)] = dot(left, w_full[k]).astype(BF16)

    row_peers(lambda r: to_row(*first_trip, r).wait_send())
    row_peers(lambda r: to_row(*second_trip, r).wait_send())
    row_peers(lambda r: to_row(*back_trip, r).wait_send())
    col_peers(lambda c: to_col(*last_trip, c).wait_send())
    col_peers(lambda c: weights_to(c).wait_send())


def body(
    tokens, w_value, w_first, w_second, w_gate, conv_taps, filter_embed, filter_freq, filter_proj, filter_decay,
    skip_gain, w_out,
):
    consts = [jnp.asarray(c) for c in constants()]
    vmem = pltpu.VMEM
    sem = pltpu.SemaphoreType.DMA
    scratch = [
        vmem((256, 2048), BF16),
        vmem((4, 2048, 64), BF16),
        vmem((3, 3, 64), F32),
        vmem((FEATS, 64), F32),
        vmem((1, 64), F32),
        vmem((64, 2, 2, 64), F32),
        vmem((2, 2, 64), F32),
        vmem((2, 64), F32),
        vmem((128, 192), BF16),
        vmem((64, 384), BF16),
        vmem((2, 64, 128), F32),
        vmem((2, 256, 256), BF16),
        vmem((2, 256, 256), BF16),
        vmem((128, LENGTH), BF16),
        vmem((2, 1024, 1024), BF16),
        vmem((3, 128, 128), F32),
        vmem((512, 128), F32),
        vmem((2, 128, 256), F32),
        vmem((256, 128), F32),
        vmem((ROWS, 8, 128), BF16),
        vmem((ROWS, 8, 128), BF16),
        vmem((ROWS, 8, 128), BF16),
        vmem((ROWS, 8, 128), BF16),
        vmem((256, 128), F32),
        vmem((ROWS, 4, 128), BF16),
        vmem((ROWS, 4, 128), BF16),
        vmem((128, 128), F32),
        vmem((COLS, 16, 128), BF16),
        vmem((COLS, 16, 128), BF16),
        sem((18,)),
        sem((ROWS,)), sem((ROWS,)), sem((ROWS,)), sem((ROWS,)), sem((ROWS,)), sem((ROWS,)),
        sem((COLS,)), sem((COLS,)), sem((COLS,)), sem((COLS,)),
        sem, sem,
    ]
    anywhere = pl.BlockSpec(memory_space=pl.ANY)
    return pl.pallas_call(
        kernel,
        out_shape=jax.ShapeDtypeStruct((1, 16, 2048), BF16),
        in_specs=[anywhere] * 18,
        out_specs=pl.BlockSpec(memory_space=pltpu.VMEM),
        scratch_shapes=scratch,
        compiler_params=pltpu.CompilerParams(
            collective_id=0, has_side_effects=True, vmem_limit_bytes=48 * 1024 * 1024
        ),
    )(
        tokens, w_value, w_first, w_second, w_gate, conv_taps, filter_embed, filter_freq.reshape(1, -1),
        filter_proj, filter_decay, skip_gain, w_out, *consts,
    )


def solution(mesh):
    placed = (
        P(None, "row", None),
        P(None, "col"),
        P(None, "col"),
        P(None, "col"),
        P(None, "col"),
        P(None, None, "col"),
        P(),
        P(),
        P(None, None, None, "col"),
        P(None, None, "col"),
        P(None, "col"),
        P("col", None),
    )
    return jax.shard_map(
        body, mesh=mesh, in_specs=placed, out_specs=P(None, ("row", "col"), None), check_vma=False
    )
```

profile of v0, /device:TPU:1, one launch (start us, length us, event | category | flops | bytes accessed | tf_op | source)
XLA Modules:
  0.0 70.1 jit_solution(12844931725260162551)
XLA Ops:
  0.0 0.0 copy-start.1
  0.0 0.0 copy-start.11
  0.0 0.0 copy-start.10
  0.0 0.0 copy-start.4
  0.0 0.0 copy-start.9
  0.0 0.0 copy-start
  0.0 1.3 %copy.19.w_value = bf16[2048,64]{1,0:T(8,128)(2,1)S(1)} copy(bf16[2048,64]{0,1:T(8,128)(2,1)} %param.19) | data formatting | bytes 524288 | tf_op args[1]
  1.4 1.2 %copy.20.w_first = bf16[2048,64]{1,0:T(8,128)(2,1)S(1)} copy(bf16[2048,64]{0,1:T(8,128)(2,1)} %param.20) | data formatting | bytes 524288 | tf_op args[2]
  2.6 1.2 %copy.21.w_second = bf16[2048,64]{1,0:T(8,128)(2,1)S(1)} copy(bf16[2048,64]{0,1:T(8,128)(2,1)} %param.21) | data formatting | bytes 524288 | tf_op args[3]
  3.8 1.2 %copy.22.w_gate = bf16[2048,64]{1,0:T(8,128)(2,1)S(1)} copy(bf16[2048,64]{0,1:T(8,128)(2,1)} %param.22) | data formatting | bytes 524288 | tf_op args[4]
  5.1 0.0 copy-done.1
  5.1 0.0 copy-done.11
  5.1 0.0 copy-done.10
  5.1 0.0 copy-done.4
  5.1 0.0 copy-done.9
  5.1 0.0 copy-done
  5.1 0.0 copy-start.2
  5.1 0.9 %copy-done.2 = bf16[2,256,256]{2,1,0:T(8,128)(2,1)S(1)} copy-done((bf16[2,256,256]{2,1,0:T(8,128)(2,1)S(1)}, bf16[2,256,256]{2,1,0:T(8,128)(2,1)}, u32[]{:S(2)}) %copy-start.2) | copy-done | bytes 262168
  6.1 0.0 copy-start.3
  6.1 0.9 %copy-done.3 = bf16[2,256,256]{2,1,0:T(8,128)(2,1)S(1)} copy-done((bf16[2,256,256]{2,1,0:T(8,128)(2,1)S(1)}, bf16[2,256,256]{2,1,0:T(8,128)(2,1)}, u32[]{:S(2)}) %copy-start.3) | copy-done | bytes 262168
  7.0 0.0 copy-start.5
  7.0 0.8 %copy-done.5 = f32[2,64,128]{2,1,0:T(8,128)S(1)} copy-done((f32[2,64,128]{2,1,0:T(8,128)S(1)}, f32[2,64,128]{2,1,0:T(8,128)}, u32[]{:S(2)}) %copy-start.5) | copy-done | bytes 65560
  7.9 0.0 copy-start.6
  7.9 0.8 %copy-done.6 = bf16[128,192]{1,0:T(8,128)(2,1)S(1)} copy-done((bf16[128,192]{1,0:T(8,128)(2,1)S(1)}, bf16[128,192]{1,0:T(8,128)(2,1)}, u32[]{:S(2)}) %copy-start.6) | copy-done | bytes 49176
  8.7 0.0 copy-start.7
  8.7 0.8 %copy-done.7 = bf16[64,384]{1,0:T(8,128)(2,1)S(1)} copy-done((bf16[64,384]{1,0:T(8,128)(2,1)S(1)}, bf16[64,384]{1,0:T(8,128)(2,1)}, u32[]{:S(2)}) %copy-start.7) | copy-done | bytes 49176
  9.5 0.0 copy-start.8
  9.5 0.7 %copy-done.8 = f32[33,64]{1,0:T(8,128)S(1)} copy-done((f32[33,64]{1,0:T(8,128)S(1)}, f32[33,64]{1,0:T(8,128)}, u32[]{:S(2)}) %copy-start.8) | copy-done | bytes 8472
  10.2 0.0 copy-start.12
  10.2 0.7 copy-done.12
  10.9 58.5 %shard_map.172 = bf16[1,16,2048]{2,1,0:T(8,128)(2,1)S(1)} custom-call(bf16[1,256,2048]{2,1,0:T(8,128)(2,1)S(1)} %copy-done, bf16[2048,64]{1,0:T(8,128)(2,1)S(1)} %copy.19.w_value, bf16[2048,64]{1,0:T(8,128)(2,1)S(1)} %copy.20.w_first, bf16[2048,64]{1,0:T(8,128)(2,1)S(1)} %copy.21.w_second, bf16[2048,64]{1,0:T(8,128)(2,1)S(1)} %copy.22.w_gate, ...), custom_call_target="tpu_custom_call" | custom-call | tf_op jit(solution)/shard_map/pallas_call | solution.py:468
  69.5 0.6 copy.24
Async XLA Ops:
  0.0 5.1 %copy-start.1 = (bf16[64,2048]{1,0:T(8,128)(2,1)S(1)}, bf16[64,2048]{1,0:T(8,128)(2,1)}, u32[]{:S(2)}) copy-start(bf16[64,2048]{1,0:T(8,128)(2,1)} %w_out.1) | copy-start | bytes 786436
  0.0 5.1 %copy-start.11 = (f32[2,64]{1,0:T(2,128)S(1)}, f32[2,64]{1,0:T(2,128)}, u32[]{:S(2)}) copy-start(f32[2,64]{1,0:T(2,128)} %gain.1) | copy-start | bytes 1540
  0.0 5.1 %copy-start.10 = (f32[2,2,64]{2,1,0:T(2,128)S(1)}, f32[2,2,64]{2,1,0:T(2,128)}, u32[]{:S(2)}) copy-start(f32[2,2,64]{2,1,0:T(2,128)} %decay.1) | copy-start | bytes 3076
  0.0 5.1 %copy-start.4 = (f32[64,2,2,64]{3,2,1,0:T(2,128)S(1)}, f32[64,2,2,64]{3,2,1,0:T(2,128)}, u32[]{:S(2)}) copy-start(f32[64,2,2,64]{3,2,1,0:T(2,128)} %proj.1) | copy-start | bytes 196612
  0.0 5.1 %copy-start.9 = (f32[3,3,64]{2,1,0:T(4,128)S(1)}, f32[3,3,64]{2,1,0:T(4,128)}, u32[]{:S(2)}) copy-start(f32[3,3,64]{2,1,0:T(4,128)} %conv_taps.1) | copy-start | bytes 6916
  0.0 5.1 %copy-start = (bf16[1,256,2048]{2,1,0:T(8,128)(2,1)S(1)}, bf16[1,256,2048]{2,1,0:T(8,128)(2,1)}, u32[]{:S(2)}) copy-start(bf16[1,256,2048]{2,1,0:T(8,128)(2,1)} %tokens.1) | copy-start | bytes 3145732
  5.1 1.0 %copy-start.2 = (bf16[2,256,256]{2,1,0:T(8,128)(2,1)S(1)}, bf16[2,256,256]{2,1,0:T(8,128)(2,1)}, u32[]{:S(2)}) copy-start(bf16[2,256,256]{2,1,0:T(8,128)(2,1)} %constant.16.clone.inner_out_h) | copy-start | bytes 786436
  6.1 0.9 %copy-start.3 = (bf16[2,256,256]{2,1,0:T(8,128)(2,1)S(1)}, bf16[2,256,256]{2,1,0:T(8,128)(2,1)}, u32[]{:S(2)}) copy-start(bf16[2,256,256]{2,1,0:T(8,128)(2,1)} %constant.15.clone.inner_in_h) | copy-start | bytes 786436
  7.0 0.8 %copy-start.5 = (f32[2,64,128]{2,1,0:T(8,128)S(1)}, f32[2,64,128]{2,1,0:T(8,128)}, u32[]{:S(2)}) copy-start(f32[2,64,128]{2,1,0:T(8,128)} %constant.14.clone.twist_h) | copy-start | bytes 196612
  7.9 0.8 %copy-start.6 = (bf16[128,192]{1,0:T(8,128)(2,1)S(1)}, bf16[128,192]{1,0:T(8,128)(2,1)}, u32[]{:S(2)}) copy-start(bf16[128,192]{1,0:T(8,128)(2,1)} %constant.12.clone.outer_in_h) | copy-start | bytes 147460
  8.7 0.8 %copy-start.7 = (bf16[64,384]{1,0:T(8,128)(2,1)S(1)}, bf16[64,384]{1,0:T(8,128)(2,1)}, u32[]{:S(2)}) copy-start(bf16[64,384]{1,0:T(8,128)(2,1)} %constant.13.clone.outer_out_h) | copy-start | bytes 147460
  9.5 0.7 %copy-start.8 = (f32[33,64]{1,0:T(8,128)S(1)}, f32[33,64]{1,0:T(8,128)}, u32[]{:S(2)}) copy-start(f32[33,64]{1,0:T(8,128)} %embed.1) | copy-start | bytes 25348
  10.2 0.7 copy-start.12
where the time goes:
time: 70.7 us; the launch traced here: 70.1 us
  Pallas kernels  58.5 us (83%)
  local copies, waits for them, and re-layouts  11.4 us (16%)
    pallas_call x1, Pallas kernels, body(): pl.pallas_call(kernel, out_shape=jax.ShapeDtypeStruct((1, 16, 2048), BF16...  58.5 us
    unnamed x31, local copies, waits for them, and re-layouts  11.4 us

commit v1 on v0

--- a/solution.py
+++ b/solution.py
@@ -160,6 +160,8 @@
     z = lax.div(row, 2)
     core = lax.rem(row, 2)
     partner = z * 2 + 1 - core
+    y = lax.div(col, 4)
+    x = lax.rem(col, 4)
 
     def row_peers(visit):
         def step(i, carry):
@@ -183,15 +185,15 @@
     row_peers(lambda r: pl.semaphore_signal(barrier, inc=1, device_id=(r, col), device_id_type=MESH))
     col_peers(lambda c: pl.semaphore_signal(barrier, inc=1, device_id=(row, c), device_id_type=MESH))
 
-    own_rows = pl.ds(pl.multiple_of(col * 64, 64), 64)
     loads = []
     for source, target in (
         (tokens.at[0], tok_v),
-        (w_value, w_v.at[0]),
-        (w_first, w_v.at[1]),
-        (w_second, w_v.at[2]),
-        (w_gate, w_v.at[3]),
-        (w_out.at[:, pl.ds(pl.multiple_of(core * 1024, 1024), 1024)], w_full.at[core, own_rows]),
+        (w_value, w_v.at[pl.ds(0, 64)]),
+        (w_first, w_v.at[pl.ds(64, 64)]),
+        (w_second, w_v.at[pl.ds(128, 64)]),
+        (w_gate, w_v.at[pl.ds(192, 64)]),
+        (w_out.at[:, pl.ds(pl.multiple_of(core * 1024, 512), 512)], w_full.at[core, 0, y, x]),
+        (w_out.at[:, pl.ds(pl.multiple_of(core * 1024 + 512, 512), 512)], w_full.at[core, 1, y, x]),
         (conv_taps, taps_v),
         (embed, embed_v),
         (freq, freq_v),
@@ -211,24 +213,24 @@
 
     for load in loads[:5]:
         load.wait()
-    order = lax.broadcasted_iota(jnp.int32, (256, 64), 0)
-    channel = lax.broadcasted_iota(jnp.int32, (256, 64), 1)
-    own_channel = channel == 2 * (order >> 3) + ((order >> 1) & 1)
-    place = [
-        jnp.where(own_channel & ((order & 1) == h) & (((order >> 2) & 1) == k), 1.0, 0.0).astype(BF16)
-        for k in range(2)
-        for h in range(2)
+    result = dot_nt(w_v[...], tok_v[...]).astype(BF16)
+    order = lax.broadcasted_iota(jnp.int32, (256, 256), 0)
+    source = lax.broadcasted_iota(jnp.int32, (256, 256), 1)
+    match = ((order >> 2) & 1) * 128 + (order & 1) * 64 + 2 * (order >> 3) + ((order >> 1) & 1)
+    place = jnp.where(source == match, 1.0, 0.0).astype(BF16)
+    parts = [
+        jnp.concatenate(
+            [result[64 * k : 64 * (k + 1), 128 * h : 128 * (h + 1)] for k in (pair, pair + 1) for h in range(2)], axis=0
+        )
+        for pair in (0, 2)
     ]
-    for pair, target in ((0, send1), (2, send2)):
-        total = jnp.zeros((256, 128), F32)
-        for k in range(2):
-            result = dot(tok_v[...], w_v[pair + k]).astype(BF16)
-            for h in range(2):
-                total = total + dot_nt(place[2 * k + h], result[128 * h : 128 * (h + 1)])
-        target[...] = total.reshape(ROWS, 8, 128).astype(BF16)
+    sorted_rows = dot(place, jnp.concatenate(parts, axis=1))
+    send1[...] = sorted_rows[:, :128].reshape(ROWS, 8, 128).astype(BF16)
+    send2[...] = sorted_rows[:, 128:].reshape(ROWS, 8, 128).astype(BF16)
     recv1[pl.ds(row, 1)] = send1[pl.ds(row, 1)]
     recv2[pl.ds(row, 1)] = send2[pl.ds(row, 1)]
     loads[5].wait()
+    loads[6].wait()
 
     def to_row(source, target, sent, received, r):
         return pltpu.make_async_remote_copy(
@@ -254,20 +256,33 @@
             device_id=(row, c), device_id_type=MESH,
         )
 
-    def weight_rows(c):
-        return w_full.at[core, pl.ds(pl.multiple_of(c * 64, 64), 64)]
-
-    def weights_to(c):
+    def along_x(i):
+        return lax.rem(x + i, 4)
+
+    def along_y(i):
+        return lax.rem(y + i, 4)
+
+    def gather(leg, part, i, sending):
+        by_x = leg == part
+        other = along_x(i) if by_x else along_y(i)
+        device = y * 4 + other if by_x else other * 4 + x
+        if leg == 0:
+            here, there = w_full.at[core, part, y, x], w_full.at[core, part, y if by_x else other, other if by_x else x]
+        elif by_x:
+            here, there = w_full.at[core, part, :, x], w_full.at[core, part, :, other]
+        else:
+            here, there = w_full.at[core, part, y], w_full.at[core, part, other]
+        slot = 2 * leg + part
         return pltpu.make_async_remote_copy(
-            src_ref=weight_rows(col), dst_ref=weight_rows(col), send_sem=send_sem5.at[c], recv_sem=recv_sem5.at[col],
-            device_id=(row, c), device_id_type=MESH,
-        )
-
-    def weights_from(c):
-        return pltpu.make_async_remote_copy(
-            src_ref=weight_rows(c), dst_ref=weight_rows(c), send_sem=send_sem5.at[c], recv_sem=recv_sem5.at[c],
-            device_id=(row, c), device_id_type=MESH,
-        )
+            src_ref=here, dst_ref=here if sending else there, send_sem=send_sem5.at[slot, other],
+            recv_sem=recv_sem5.at[slot, (x if by_x else y) if sending else other],
+            device_id=(row, device), device_id_type=MESH,
+        )
+
+    def gather_all(leg, visit):
+        for part in range(2):
+            for i in (2, 1, 3):
+                visit(part, i)
 
     first_trip = (send1, recv1, send_sem1, recv_sem1)
     second_trip = (send2, recv2, send_sem2, recv_sem2)
@@ -277,9 +292,9 @@
     pl.semaphore_wait(barrier, ROWS - 1 + COLS - 1)
     row_peers(lambda r: to_row(*first_trip, r).start())
     row_peers(lambda r: to_row(*second_trip, r).start())
-    col_peers(lambda c: weights_to(c).start())
-
-    for load in loads[6:]:
+    gather_all(0, lambda part, i: gather(0, part, i, True).start())
+
+    for load in loads[7:]:
         load.wait()
     scaled = embed_v[...] * freq_v[...]
     est[...] = jnp.zeros_like(est)
@@ -368,6 +383,9 @@
             )
         return jnp.concatenate(whole, axis=1)
 
+    gather_all(0, lambda part, i: gather(0, part, i, False).wait_recv())
+    gather_all(1, lambda part, i: gather(1, part, i, True).start())
+
     row_peers(lambda r: from_row(*first_trip, r).wait_recv())
     arrived(recv1)
     value = short(0, 0)
@@ -389,7 +407,7 @@
     recv3[pl.ds(row, 1)] = send3[pl.ds(row, 1)]
     row_peers(lambda r: to_row(*back_trip, r).start())
 
-    col_peers(lambda c: weights_from(c).wait_recv())
+    gather_all(1, lambda part, i: gather(1, part, i, False).wait_recv())
     swap = pltpu.make_async_remote_copy(
         src_ref=w_full.at[core], dst_ref=w_full.at[core], send_sem=swap_send, recv_sem=swap_recv,
         device_id=(partner, col), device_id_type=MESH,
@@ -413,13 +431,16 @@
     col_peers(lambda c: from_col(*last_trip, c).wait_recv())
     left = jnp.concatenate([recv4[2 * m] + recv4[2 * m + 1] for m in range(8)], axis=1)
     for k in range(2):
-        out_ref[0, :, 1024 * k : 1024 * (k + 1)] = dot(left, w_full[k]).astype(BF16)
+        for part in range(2):
+            at = 1024 * k + 512 * part
+            out_ref[0, :, at : at + 512] = dot(left, w_full[k, part].reshape(1024, 512)).astype(BF16)
 
     row_peers(lambda r: to_row(*first_trip, r).wait_send())
     row_peers(lambda r: to_row(*second_trip, r).wait_send())
     row_peers(lambda r: to_row(*back_trip, r).wait_send())
     col_peers(lambda c: to_col(*last_trip, c).wait_send())
-    col_peers(lambda c: weights_to(c).wait_send())
+    gather_all(0, lambda part, i: gather(0, part, i, True).wait_send())
+    gather_all(1, lambda part, i: gather(1, part, i, True).wait_send())
 
 
 def body(
@@ -431,7 +452,7 @@
     sem = pltpu.SemaphoreType.DMA
     scratch = [
         vmem((256, 2048), BF16),
-        vmem((4, 2048, 64), BF16),
+        vmem((256, 2048), BF16),
         vmem((3, 3, 64), F32),
         vmem((FEATS, 64), F32),
         vmem((1, 64), F32),
@@ -444,7 +465,7 @@
         vmem((2, 256, 256), BF16),
         vmem((2, 256, 256), BF16),
         vmem((128, LENGTH), BF16),
-        vmem((2, 1024, 1024), BF16),
+        vmem((2, 2, 4, 4, 64, 512), BF16),
         vmem((3, 128, 128), F32),
         vmem((512, 128), F32),
         vmem((2, 128, 256), F32),
@@ -459,12 +480,12 @@
         vmem((128, 128), F32),
         vmem((COLS, 16, 128), BF16),
         vmem((COLS, 16, 128), BF16),
-        sem((18,)),
+        sem((19,)),
         sem((ROWS,)), sem((ROWS,)), sem((ROWS,)), sem((ROWS,)), sem((ROWS,)), sem((ROWS,)),
-        sem((COLS,)), sem((COLS,)), sem((COLS,)), sem((COLS,)),
+        sem((COLS,)), sem((COLS,)), sem((4, 4)), sem((4, 4)),
         sem, sem,
     ]
-    anywhere = pl.BlockSpec(memory_space=pl.ANY)
+    anywhere = pl.BlockSpec(memory_space=pltpu.HBM)
     return pl.pallas_call(
         kernel,
         out_shape=jax.ShapeDtypeStruct((1, 16, 2048), BF16),
@@ -472,10 +493,10 @@
         out_specs=pl.BlockSpec(memory_space=pltpu.VMEM),
         scratch_shapes=scratch,
         compiler_params=pltpu.CompilerParams(
-            collective_id=0, has_side_effects=True, vmem_limit_bytes=48 * 1024 * 1024
+            collective_id=0, has_side_effects=True, vmem_limit_bytes=67043328
         ),
     )(
-        tokens, w_value, w_first, w_second, w_gate, conv_taps, filter_embed, filter_freq.reshape(1, -1),
+        tokens, w_value.T, w_first.T, w_second.T, w_gate.T, conv_taps, filter_embed, filter_freq.reshape(1, -1),
         filter_proj, filter_decay, skip_gain, w_out, *consts,
     )
 

time: 70.7 us -> 48.2 us (0.68)
  Pallas kernels: 58.5 us -> 46.6 us
  local copies, waits for them, and re-layouts: 11.4 us -> 1.47 us
    pallas_call x1, Pallas kernels: 58.5 us -> 46.6 us  [body(): pl.pallas_call(kernel, out_shape=jax.ShapeDtypeStruct((1, 16, 2048), BF16...]
    unnamed x31 -> x1, local copies, waits for them, and re-layouts: 11.4 us -> 1.47 us
where the time goes in v1:
time: 48.2 us; the launch traced here: 48.1 us
  Pallas kernels  46.6 us (97%)
  local copies, waits for them, and re-layouts  1.47 us (3%)
    pallas_call x1, Pallas kernels, body(): pl.pallas_call(kernel, out_shape=jax.ShapeDtypeStruct((1, 16, 2048), BF16...  46.6 us
    unnamed x1, local copies, waits for them, and re-layouts  1.47 us

profile of v1, /device:TPU:1, one launch (start us, length us, event | category | flops | bytes accessed | tf_op | source)
XLA Modules:
  0.0 48.1 jit_solution(12804339324060321844)
XLA Ops:
  0.0 46.6 %shard_map.172 = bf16[1,16,2048]{2,1,0:T(8,128)(2,1)} custom-call(bf16[1,256,2048]{2,1,0:T(8,128)(2,1)} %tokens.1, bf16[64,2048]{1,0:T(8,128)(2,1)} %bitcast.5, bf16[64,2048]{1,0:T(8,128)(2,1)} %bitcast.6, bf16[64,2048]{1,0:T(8,128)(2,1)} %bitcast.7, bf16[64,2048]{1,0:T(8,128)(2,1)} %bitcast.8, f32[3,3,64]{2,1,0:T(4,128)} %conv_taps.1, f32[33,64]{1,0:T(8,128)} %embed.1, ...), custom_call_target="tpu_custom_call" | custom-call | tf_op jit(solution)/shard_map/pallas_call | solution.py:489
  46.6 1.5 %copy.20 = bf16[1,16,2048]{2,1,0:T(8,128)(2,1)} copy(bf16[1,16,2048]{2,1,0:T(8,128)(2,1)} %shard_map.172) | data formatting | bytes 131072

commit v2 on v1

--- a/solution.py
+++ b/solution.py
@@ -151,9 +151,10 @@
     out_ref,
     tok_v, w_v, taps_v, embed_v, freq_v, proj_v, decay_v, gain_v,
     outer_in_v, outer_out_v, twist_v, inner_in_v, inner_out_v, table_v,
-    w_full, est, lag_taps, spectra, grid_v, send1, recv1, send2, recv2, back_v, send3, recv3, block_v, send4, recv4,
+    w_full, est, lag_taps, spectra, sort_v, gate_v, block_v, back_v, edge_out, edge_in,
+    send1, recv1, send2, recv2, send3, recv3, send4, recv4,
     load_sem, send_sem1, recv_sem1, send_sem2, recv_sem2, send_sem3, recv_sem3, send_sem4, recv_sem4,
-    send_sem5, recv_sem5, swap_send, swap_recv,
+    edge_send, edge_recv, block_send, block_recv, hop_send, hop_recv, swap_send, swap_recv,
 ):
     row = lax.axis_index("row")
     col = lax.axis_index("col")
@@ -214,85 +215,115 @@
     for load in loads[:5]:
         load.wait()
     result = dot_nt(w_v[...], tok_v[...]).astype(BF16)
-    order = lax.broadcasted_iota(jnp.int32, (256, 256), 0)
-    source = lax.broadcasted_iota(jnp.int32, (256, 256), 1)
-    match = ((order >> 2) & 1) * 128 + (order & 1) * 64 + 2 * (order >> 3) + ((order >> 1) & 1)
-    place = jnp.where(source == match, 1.0, 0.0).astype(BF16)
-    parts = [
-        jnp.concatenate(
-            [result[64 * k : 64 * (k + 1), 128 * h : 128 * (h + 1)] for k in (pair, pair + 1) for h in range(2)], axis=0
-        )
-        for pair in (0, 2)
+    order = lax.broadcasted_iota(jnp.int32, (128, 128), 0)
+    source = lax.broadcasted_iota(jnp.int32, (128, 128), 1)
+    place = jnp.where(source == (order & 1) * 64 + (order >> 1), 1.0, 0.0).astype(BF16)
+    roles = [
+        jnp.concatenate([result[64 * k : 64 * (k + 1), :128], result[64 * k : 64 * (k + 1), 128:]], axis=0)
+        for k in range(4)
     ]
-    sorted_rows = dot(place, jnp.concatenate(parts, axis=1))
-    send1[...] = sorted_rows[:, :128].reshape(ROWS, 8, 128).astype(BF16)
-    send2[...] = sorted_rows[:, 128:].reshape(ROWS, 8, 128).astype(BF16)
+    sort_v[...] = dot(place, jnp.concatenate(roles, axis=1))
+    for r in range(ROWS):
+        send1[r] = sort_v[4 * r : 4 * r + 4, :128].astype(BF16)
+        send2[r] = sort_v[4 * r : 4 * r + 4, 128:256].astype(BF16)
     recv1[pl.ds(row, 1)] = send1[pl.ds(row, 1)]
     recv2[pl.ds(row, 1)] = send2[pl.ds(row, 1)]
+    end_row = lax.broadcasted_iota(jnp.int32, (16, 256), 0)
+    end_col = lax.broadcasted_iota(jnp.int32, (16, 256), 1)
+    ends = jnp.where(end_col == 255 * end_row, 1.0, 0.0).astype(BF16)
+    edge_out[...] = dot_nt(ends, result[128:]).astype(BF16)
     loads[5].wait()
     loads[6].wait()
 
-    def to_row(source, target, sent, received, r):
-        return pltpu.make_async_remote_copy(
-            src_ref=source.at[r], dst_ref=target.at[row], send_sem=sent.at[r], recv_sem=received.at[row],
+    def to_row(trip, r):
+        source, target, sent, received = trip
+        return pltpu.make_async_remote_copy(
+            src_ref=source.at[r], dst_ref=target.at[row], send_sem=sent, recv_sem=received,
             device_id=(r, col), device_id_type=MESH,
         )
 
-    def from_row(source, target, sent, received, r):
-        return pltpu.make_async_remote_copy(
-            src_ref=source.at[r], dst_ref=target.at[r], send_sem=sent.at[r], recv_sem=received.at[r],
-            device_id=(r, col), device_id_type=MESH,
-        )
-
-    def to_col(source, target, sent, received, c):
-        return pltpu.make_async_remote_copy(
-            src_ref=source.at[c], dst_ref=target.at[col], send_sem=sent.at[c], recv_sem=received.at[col],
+    def to_col(trip, c):
+        source, target, sent, received = trip
+        return pltpu.make_async_remote_copy(
+            src_ref=source.at[c], dst_ref=target.at[col], send_sem=sent, recv_sem=received,
             device_id=(row, c), device_id_type=MESH,
         )
 
-    def from_col(source, target, sent, received, c):
-        return pltpu.make_async_remote_copy(
-            src_ref=source.at[c], dst_ref=target.at[c], send_sem=sent.at[c], recv_sem=received.at[c],
-            device_id=(row, c), device_id_type=MESH,
-        )
-
-    def along_x(i):
-        return lax.rem(x + i, 4)
-
-    def along_y(i):
-        return lax.rem(y + i, 4)
-
-    def gather(leg, part, i, sending):
-        by_x = leg == part
-        other = along_x(i) if by_x else along_y(i)
-        device = y * 4 + other if by_x else other * 4 + x
-        if leg == 0:
-            here, there = w_full.at[core, part, y, x], w_full.at[core, part, y if by_x else other, other if by_x else x]
-        elif by_x:
-            here, there = w_full.at[core, part, :, x], w_full.at[core, part, :, other]
-        else:
-            here, there = w_full.at[core, part, y], w_full.at[core, part, other]
-        slot = 2 * leg + part
-        return pltpu.make_async_remote_copy(
-            src_ref=here, dst_ref=here if sending else there, send_sem=send_sem5.at[slot, other],
-            recv_sem=recv_sem5.at[slot, (x if by_x else y) if sending else other],
-            device_id=(row, device), device_id_type=MESH,
-        )
-
-    def gather_all(leg, visit):
-        for part in range(2):
-            for i in (2, 1, 3):
-                visit(part, i)
-
-    first_trip = (send1, recv1, send_sem1, recv_sem1)
-    second_trip = (send2, recv2, send_sem2, recv_sem2)
+    def whole(trip):
+        source, target, sent, received = trip
+        count = pl.ds(0, source.shape[0] - 1)
+        return pltpu.make_async_remote_copy(
+            src_ref=source.at[count], dst_ref=target.at[count], send_sem=sent, recv_sem=received,
+            device_id=(partner, col), device_id_type=MESH,
+        )
+
+    def edge(step, slot):
+        return pltpu.make_async_remote_copy(
+            src_ref=edge_out, dst_ref=edge_in.at[slot], send_sem=edge_send.at[slot], recv_sem=edge_recv.at[slot],
+            device_id=(lax.rem(row + step, ROWS), col), device_id_type=MESH,
+        )
+
+    after_me, before_me = edge(1, 0), edge(ROWS - 1, 1)
+
+    def block(part, yy, xx):
+        return w_full.at[core, part, yy, xx]
+
+    def group(part, step, half=None):
+        some = slice(None) if half is None else pl.ds(2 * half, 2)
+        if part == 0:
+            return w_full.at[core, 0, lax.rem(y + step, 4), some]
+        return w_full.at[core, 1, some, lax.rem(x + step, 4)]
+
+    def across(part, step):
+        return lax.rem(y + step, 4) * 4 + x if part == 0 else y * 4 + lax.rem(x + step, 4)
+
+    def spread_block(part, step):
+        there = y * 4 + lax.rem(x + step, 4) if part == 0 else lax.rem(y + step, 4) * 4 + x
+        return pltpu.make_async_remote_copy(
+            src_ref=block(part, y, x), dst_ref=block(part, y, x), send_sem=block_send.at[part],
+            recv_sem=block_recv.at[part], device_id=(row, there), device_id_type=MESH,
+        )
+
+    def blocks(part):
+        three = w_full.at[core, part, 0, pl.ds(0, 3)]
+        return pltpu.make_async_remote_copy(
+            src_ref=three, dst_ref=three, send_sem=block_send.at[part], recv_sem=block_recv.at[part],
+            device_id=(partner, col), device_id_type=MESH,
+        )
+
+    def hop(part, step, held, half=None):
+        side = (0 if half is None else 2) + (0 if step == 1 else 1)
+        here = group(part, held, half)
+        return pltpu.make_async_remote_copy(
+            src_ref=here, dst_ref=here, send_sem=hop_send.at[part, side], recv_sem=hop_recv.at[part, side],
+            device_id=(row, across(part, step)), device_id_type=MESH,
+        )
+
+    def hops(half):
+        if half:
+            return [hop(part, step, 4 - step, 0 if step == 1 else 1) for part in range(2) for step in (1, 3)]
+        return [hop(part, step, 0) for part in range(2) for step in (1, 3)]
+
+    def swap(part, step):
+        here = group(part, step)
+        return pltpu.make_async_remote_copy(
+            src_ref=here, dst_ref=here, send_sem=swap_send, recv_sem=swap_recv,
+            device_id=(partner, col), device_id_type=MESH,
+        )
+
+    value_trip = (send1, recv1, send_sem1, recv_sem1)
+    first_trip = (send2, recv2, send_sem2, recv_sem2)
     back_trip = (send3, recv3, send_sem3, recv_sem3)
     last_trip = (send4, recv4, send_sem4, recv_sem4)
 
     pl.semaphore_wait(barrier, ROWS - 1 + COLS - 1)
-    row_peers(lambda r: to_row(*first_trip, r).start())
-    row_peers(lambda r: to_row(*second_trip, r).start())
-    gather_all(0, lambda part, i: gather(0, part, i, True).start())
+    row_peers(lambda r: to_row(value_trip, r).start())
+    for part in range(2):
+        for step in (2, 1, 3):
+            spread_block(part, step).start()
+    row_peers(lambda r: to_row(first_trip, r).start())
+    after_me.start()
+    before_me.start()
 
     for load in loads[7:]:
         load.wait()
@@ -361,86 +392,115 @@
         spectra[o] = filter_spectrum(signals, outer_in_v[...], twist, inner_in)
     tables = (outer_in_v[...], outer_out_v[...], twist, inner_in, inner_out)
 
+    for part in range(2):
+        blocks(part).wait_recv()
+    first_hops, second_hops = hops(False), hops(True)
+    for copy in first_hops:
+        copy.start()
+    for part in range(2):
+        swap(part, 0).start()
+
+    lane = lax.broadcasted_iota(jnp.int32, (128, 128), 1)
+    sub = lax.broadcasted_iota(jnp.int32, (128, 128), 0)
+    upper = (sub & 1) == 1
+    after_me.wait_recv()
+    before_me.wait_recv()
+    double = jnp.where(lane == (sub >> 1), 1.0, 0.0)
+    edge_before = dot_nt(double.astype(BF16), edge_in[0])[:, 1:2]
+    edge_after = dot_nt(double.astype(BF16), edge_in[1])[:, 0:1]
+    edge_before = jnp.where(row == 0, 0.0, edge_before)
+    edge_after = jnp.where(row == ROWS - 1, 0.0, edge_after)
+    role_taps = jnp.concatenate([taps_v[j, 2:3] for j in range(3)] + [jnp.zeros((5, 64), F32)], axis=0)
+    columns = dot_nt(double[:, :64], role_taps, lax.Precision.HIGHEST)
+    here = sort_v[:, 256:384]
+    right, left = pltpu.roll(here, 1, 1), pltpu.roll(here, 127, 1)
+    before = jnp.where(lane == 0, jnp.where(upper, pltpu.roll(right, 1, 0), edge_before), right)
+    after = jnp.where(lane == 127, jnp.where(upper, edge_after, pltpu.roll(left, 127, 0)), left)
+    second = before * columns[:, 0:1] + here * columns[:, 1:2] + after * columns[:, 2:3]
+    gate = sort_v[:, 384:]
+    gate_v[...] = second * (gate / (1.0 + jnp.exp(-gate)))
+
     lane = lax.broadcasted_iota(jnp.int32, (32, 128), 1)
     sub = lax.broadcasted_iota(jnp.int32, (32, 128), 0)
 
     def arrived(buffer):
-        grid_v[...] = buffer[...].astype(F32).reshape(ROWS * 8, 128)
-
-    def loaded(k, c):
-        return [grid_v[pl.ds(4 * k + 2 * c + h, 32, stride=8), :] for h in range(2)]
-
-    def short(k, role):
-        whole = []
+        for r in range(ROWS):
+            block_v[4 * r : 4 * r + 4, :] = buffer[r].astype(F32)
+
+    def short(role):
+        sides = []
         for c in range(2):
-            here = loaded(k, c)
+            here = [block_v[pl.ds(2 * c + h, 32, stride=4), :] for h in range(2)]
             before, after = shifted(here, lane, sub)
             weight = [own_taps[c][j, role : role + 1] for j in range(3)]
-            whole.append(
+            sides.append(
                 jnp.concatenate(
                     [before[h] * weight[0] + here[h] * weight[1] + after[h] * weight[2] for h in range(2)], axis=0
                 )
             )
-        return jnp.concatenate(whole, axis=1)
-
-    gather_all(0, lambda part, i: gather(0, part, i, False).wait_recv())
-    gather_all(1, lambda part, i: gather(1, part, i, True).start())
-
-    row_peers(lambda r: from_row(*first_trip, r).wait_recv())
+        return jnp.concatenate(sides, axis=1)
+
+    whole(value_trip).wait_recv()
     arrived(recv1)
-    value = short(0, 0)
-    first = short(1, 1)
-    inner = first * convolve(value, spectra[0], tables)
-    second_conv = convolve(inner, spectra[1], tables)
-
-    row_peers(lambda r: from_row(*second_trip, r).wait_recv())
+    conv = convolve(short(0), spectra[0], tables)
+    whole(first_trip).wait_recv()
     arrived(recv2)
-    second = short(0, 2)
-    gate = jnp.concatenate([jnp.concatenate(loaded(1, c), axis=0) for c in range(2)], axis=1)
-    outer = second * second_conv * (gate / (1.0 + jnp.exp(-gate)))
+    conv = convolve(short(1) * conv, spectra[1], tables)
 
     for c in range(2):
         for h in range(2):
-            back_v[pl.ds(2 * c + h, 32, stride=8), :] = outer[32 * h : 32 * (h + 1), 128 * c : 128 * (c + 1)]
+            back_v[pl.ds(2 * c + h, 32, stride=4), :] = conv[32 * h : 32 * (h + 1), 128 * c : 128 * (c + 1)]
     for r in range(ROWS):
-        send3[r] = back_v[8 * r : 8 * r + 4, :].astype(BF16)
+        send3[r] = back_v[4 * r : 4 * r + 4, :].astype(BF16)
     recv3[pl.ds(row, 1)] = send3[pl.ds(row, 1)]
-    row_peers(lambda r: to_row(*back_trip, r).start())
-
-    gather_all(1, lambda part, i: gather(1, part, i, False).wait_recv())
-    swap = pltpu.make_async_remote_copy(
-        src_ref=w_full.at[core], dst_ref=w_full.at[core], send_sem=swap_send, recv_sem=swap_recv,
-        device_id=(partner, col), device_id_type=MESH,
-    )
-    swap.start()
-
-    row_peers(lambda r: from_row(*back_trip, r).wait_recv())
-    for r in range(ROWS):
-        block_v[4 * r : 4 * r + 4, :] = recv3[r].astype(F32)
-    flipped = jnp.transpose(block_v[...]).astype(BF16)
+    row_peers(lambda r: to_row(back_trip, r).start())
+
+    for copy in first_hops:
+        copy.wait_recv()
+    for copy in second_hops:
+        copy.start()
+    for part in range(2):
+        for step in (1, 3):
+            swap(part, step).start()
+
     i128 = lax.broadcasted_iota(jnp.int32, (128, 256), 0)
     l256 = lax.broadcasted_iota(jnp.int32, (128, 256), 1)
     spread = jnp.where(l256 == 128 * (i128 & 1) + 64 * lax.rem(col, 2) + (i128 >> 1), 1.0, 0.0).astype(BF16)
+    whole(back_trip).wait_recv()
+    arrived(recv3)
+    flipped = jnp.transpose(block_v[...] * gate_v[...]).astype(BF16)
     rows = dot(flipped, spread).astype(BF16)
     for h in range(2):
         send4[8 * h : 8 * (h + 1)] = rows[:, 128 * h : 128 * (h + 1)].reshape(8, 16, 128)
     recv4[pl.ds(col, 1)] = send4[pl.ds(col, 1)]
-    col_peers(lambda c: to_col(*last_trip, c).start())
-
-    swap.wait()
-    col_peers(lambda c: from_col(*last_trip, c).wait_recv())
+    col_peers(lambda c: to_col(last_trip, c).start())
+
+    for copy in second_hops:
+        copy.wait_recv()
+    for part in range(2):
+        swap(part, 2).start()
+    half = w_full.at[core]
+    swapped = pltpu.make_async_remote_copy(
+        src_ref=half, dst_ref=half, send_sem=swap_send, recv_sem=swap_recv,
+        device_id=(partner, col), device_id_type=MESH,
+    )
+    swapped.wait_recv()
+    whole(last_trip).wait_recv()
     left = jnp.concatenate([recv4[2 * m] + recv4[2 * m + 1] for m in range(8)], axis=1)
     for k in range(2):
         for part in range(2):
             at = 1024 * k + 512 * part
             out_ref[0, :, at : at + 512] = dot(left, w_full[k, part].reshape(1024, 512)).astype(BF16)
 
-    row_peers(lambda r: to_row(*first_trip, r).wait_send())
-    row_peers(lambda r: to_row(*second_trip, r).wait_send())
-    row_peers(lambda r: to_row(*back_trip, r).wait_send())
-    col_peers(lambda c: to_col(*last_trip, c).wait_send())
-    gather_all(0, lambda part, i: gather(0, part, i, True).wait_send())
-    gather_all(1, lambda part, i: gather(1, part, i, True).wait_send())
+    for trip in (value_trip, first_trip, back_trip, last_trip):
+        whole(trip).wait_send()
+    after_me.wait_send()
+    before_me.wait_send()
+    for part in range(2):
+        blocks(part).wait_send()
+    for copy in first_hops + second_hops:
+        copy.wait_send()
+    swapped.wait_send()
 
 
 def body(
@@ -469,21 +529,19 @@
         vmem((3, 128, 128), F32),
         vmem((512, 128), F32),
         vmem((2, 128, 256), F32),
-        vmem((256, 128), F32),
-        vmem((ROWS, 8, 128), BF16),
-        vmem((ROWS, 8, 128), BF16),
-        vmem((ROWS, 8, 128), BF16),
-        vmem((ROWS, 8, 128), BF16),
-        vmem((256, 128), F32),
-        vmem((ROWS, 4, 128), BF16),
-        vmem((ROWS, 4, 128), BF16),
+        vmem((128, 512), F32),
         vmem((128, 128), F32),
-        vmem((COLS, 16, 128), BF16),
-        vmem((COLS, 16, 128), BF16),
+        vmem((128, 128), F32),
+        vmem((128, 128), F32),
+        vmem((16, 128), BF16),
+        vmem((2, 16, 128), BF16),
+        vmem((ROWS, 4, 128), BF16), vmem((ROWS, 4, 128), BF16),
+        vmem((ROWS, 4, 128), BF16), vmem((ROWS, 4, 128), BF16),
+        vmem((ROWS, 4, 128), BF16), vmem((ROWS, 4, 128), BF16),
+        vmem((COLS, 16, 128), BF16), vmem((COLS, 16, 128), BF16),
         sem((19,)),
-        sem((ROWS,)), sem((ROWS,)), sem((ROWS,)), sem((ROWS,)), sem((ROWS,)), sem((ROWS,)),
-        sem((COLS,)), sem((COLS,)), sem((4, 4)), sem((4, 4)),
-        sem, sem,
+        sem, sem, sem, sem, sem, sem, sem, sem,
+        sem((2,)), sem((2,)), sem((2,)), sem((2,)), sem((2, 4)), sem((2, 4)), sem, sem,
     ]
     anywhere = pl.BlockSpec(memory_space=pltpu.HBM)
     return pl.pallas_call(

time: 48.2 us -> 43.4 us (0.900)
  Pallas kernels: 46.6 us -> 41.7 us
    pallas_call x1, Pallas kernels: 46.6 us -> 41.7 us  [body(): pl.pallas_call(kernel, out_shape=jax.ShapeDtypeStruct((1, 16, 2048), BF16...]
where the time goes in v2:
time: 43.4 us; the launch traced here: 43.2 us
  Pallas kernels  41.7 us (96%)
  local copies, waits for them, and re-layouts  1.47 us (3%)
    pallas_call x1, Pallas kernels, body(): pl.pallas_call(kernel, out_shape=jax.ShapeDtypeStruct((1, 16, 2048), BF16...  41.7 us
    unnamed x1, local copies, waits for them, and re-layouts  1.47 us

profile of v2, /device:TPU:1, one launch (start us, length us, event | category | flops | bytes accessed | tf_op | source)
XLA Modules:
  0.0 43.2 jit_solution(8859514982272046648)
XLA Ops:
  0.0 41.7 %shard_map.172 = bf16[1,16,2048]{2,1,0:T(8,128)(2,1)} custom-call(bf16[1,256,2048]{2,1,0:T(8,128)(2,1)} %tokens.1, bf16[64,2048]{1,0:T(8,128)(2,1)} %bitcast.5, bf16[64,2048]{1,0:T(8,128)(2,1)} %bitcast.6, bf16[64,2048]{1,0:T(8,128)(2,1)} %bitcast.7, bf16[64,2048]{1,0:T(8,128)(2,1)} %bitcast.8, f32[3,3,64]{2,1,0:T(4,128)} %conv_taps.1, f32[33,64]{1,0:T(8,128)} %embed.1, ...), custom_call_target="tpu_custom_call" | custom-call | tf_op jit(solution)/shard_map/pallas_call | solution.py:547
  41.7 1.5 %copy.20 = bf16[1,16,2048]{2,1,0:T(8,128)(2,1)} copy(bf16[1,16,2048]{2,1,0:T(8,128)(2,1)} %shard_map.172) | data formatting | bytes 131072

commit v3 on v2

--- a/solution.py
+++ b/solution.py
@@ -152,9 +152,9 @@
     tok_v, w_v, taps_v, embed_v, freq_v, proj_v, decay_v, gain_v,
     outer_in_v, outer_out_v, twist_v, inner_in_v, inner_out_v, table_v,
     w_full, est, lag_taps, spectra, sort_v, gate_v, block_v, back_v, edge_out, edge_in,
-    send1, recv1, send2, recv2, send3, recv3, send4, recv4,
+    send1, recv1, send2, recv2, send3, recv3, send4, recv4, total,
     load_sem, send_sem1, recv_sem1, send_sem2, recv_sem2, send_sem3, recv_sem3, send_sem4, recv_sem4,
-    edge_send, edge_recv, block_send, block_recv, hop_send, hop_recv, swap_send, swap_recv,
+    edge_send, edge_recv, block_send, block_recv, hop_send, hop_recv, pass_send, pass_recv, swap_send, swap_recv,
 ):
     row = lax.axis_index("row")
     col = lax.axis_index("col")
@@ -242,13 +242,6 @@
             device_id=(r, col), device_id_type=MESH,
         )
 
-    def to_col(trip, c):
-        source, target, sent, received = trip
-        return pltpu.make_async_remote_copy(
-            src_ref=source.at[c], dst_ref=target.at[col], send_sem=sent, recv_sem=received,
-            device_id=(row, c), device_id_type=MESH,
-        )
-
     def whole(trip):
         source, target, sent, received = trip
         count = pl.ds(0, source.shape[0] - 1)
@@ -265,8 +258,10 @@
 
     after_me, before_me = edge(1, 0), edge(ROWS - 1, 1)
 
-    def block(part, yy, xx):
-        return w_full.at[core, part, yy, xx]
+    def block(part, step):
+        if part == 0:
+            return w_full.at[core, 0, y, lax.rem(x + step, 4)]
+        return w_full.at[core, 1, lax.rem(y + step, 4), x]
 
     def group(part, step, half=None):
         some = slice(None) if half is None else pl.ds(2 * half, 2)
@@ -274,35 +269,38 @@
             return w_full.at[core, 0, lax.rem(y + step, 4), some]
         return w_full.at[core, 1, some, lax.rem(x + step, 4)]
 
-    def across(part, step):
-        return lax.rem(y + step, 4) * 4 + x if part == 0 else y * 4 + lax.rem(x + step, 4)
+    def along(part, step):
+        return y * 4 + lax.rem(x + step, 4) if part == 0 else lax.rem(y + step, 4) * 4 + x
 
     def spread_block(part, step):
-        there = y * 4 + lax.rem(x + step, 4) if part == 0 else lax.rem(y + step, 4) * 4 + x
-        return pltpu.make_async_remote_copy(
-            src_ref=block(part, y, x), dst_ref=block(part, y, x), send_sem=block_send.at[part],
-            recv_sem=block_recv.at[part], device_id=(row, there), device_id_type=MESH,
-        )
-
-    def blocks(part):
-        three = w_full.at[core, part, 0, pl.ds(0, 3)]
-        return pltpu.make_async_remote_copy(
-            src_ref=three, dst_ref=three, send_sem=block_send.at[part], recv_sem=block_recv.at[part],
-            device_id=(partner, col), device_id_type=MESH,
-        )
-
-    def hop(part, step, held, half=None):
-        side = (0 if half is None else 2) + (0 if step == 1 else 1)
-        here = group(part, held, half)
+        here = block(part, 0)
+        return pltpu.make_async_remote_copy(
+            src_ref=here, dst_ref=here, send_sem=block_send.at[part, step],
+            recv_sem=block_recv.at[part, step], device_id=(row, along(part, step)), device_id_type=MESH,
+        )
+
+    def hop_block(part, side, step):
+        here = block(part, step)
         return pltpu.make_async_remote_copy(
             src_ref=here, dst_ref=here, send_sem=hop_send.at[part, side], recv_sem=hop_recv.at[part, side],
-            device_id=(row, across(part, step)), device_id_type=MESH,
-        )
-
-    def hops(half):
-        if half:
-            return [hop(part, step, 4 - step, 0 if step == 1 else 1) for part in range(2) for step in (1, 3)]
-        return [hop(part, step, 0) for part in range(2) for step in (1, 3)]
+            device_id=(row, along(1 - part, 1 + 2 * side)), device_id_type=MESH,
+        )
+
+    def hopped(part, side):
+        here = group(part, 3 - 2 * side)
+        return pltpu.make_async_remote_copy(
+            src_ref=here, dst_ref=here, send_sem=hop_send.at[part, side], recv_sem=hop_recv.at[part, side],
+            device_id=(row, along(1 - part, 1 + 2 * side)), device_id_type=MESH,
+        )
+
+    def pass_on(part, side):
+        here = group(part, 3 - 2 * side, side)
+        return pltpu.make_async_remote_copy(
+            src_ref=here, dst_ref=here, send_sem=pass_send.at[part, side], recv_sem=pass_recv.at[part, side],
+            device_id=(row, along(1 - part, 1 + 2 * side)), device_id_type=MESH,
+        )
+
+    both = [(part, side) for part in range(2) for side in range(2)]
 
     def swap(part, step):
         here = group(part, step)
@@ -314,13 +312,15 @@
     value_trip = (send1, recv1, send_sem1, recv_sem1)
     first_trip = (send2, recv2, send_sem2, recv_sem2)
     back_trip = (send3, recv3, send_sem3, recv_sem3)
-    last_trip = (send4, recv4, send_sem4, recv_sem4)
+    last_trip = (send4, recv4, send_sem4, recv_sem4.at[0])
 
     pl.semaphore_wait(barrier, ROWS - 1 + COLS - 1)
     row_peers(lambda r: to_row(value_trip, r).start())
-    for part in range(2):
-        for step in (2, 1, 3):
+    for step in (1, 3, 2):
+        for part in range(2):
             spread_block(part, step).start()
+    for part, side in both:
+        hop_block(part, side, 0).start()
     row_peers(lambda r: to_row(first_trip, r).start())
     after_me.start()
     before_me.start()
@@ -392,13 +392,48 @@
         spectra[o] = filter_spectrum(signals, outer_in_v[...], twist, inner_in)
     tables = (outer_in_v[...], outer_out_v[...], twist, inner_in, inner_out)
 
-    for part in range(2):
-        blocks(part).wait_recv()
-    first_hops, second_hops = hops(False), hops(True)
-    for copy in first_hops:
-        copy.start()
+    for step in (1, 3, 2):
+        for part in range(2):
+            spread_block(part, step).wait_recv()
+        for part, side in both:
+            hop_block(part, side, 4 - step).start()
     for part in range(2):
         swap(part, 0).start()
+
+    lane = lax.broadcasted_iota(jnp.int32, (32, 128), 1)
+    sub = lax.broadcasted_iota(jnp.int32, (32, 128), 0)
+
+    def arrived(buffer):
+        for r in range(ROWS):
+            block_v[4 * r : 4 * r + 4, :] = buffer[r].astype(F32)
+
+    def short(role):
+        sides = []
+        for c in range(2):
+            here = [block_v[pl.ds(2 * c + h, 32, stride=4), :] for h in range(2)]
+            before, after = shifted(here, lane, sub)
+            weight = [own_taps[c][j, role : role + 1] for j in range(3)]
+            sides.append(
+                jnp.concatenate(
+                    [before[h] * weight[0] + here[h] * weight[1] + after[h] * weight[2] for h in range(2)], axis=0
+                )
+            )
+        return jnp.concatenate(sides, axis=1)
+
+    whole(value_trip).wait_recv()
+    arrived(recv1)
+    conv = convolve(short(0), spectra[0], tables)
+    whole(first_trip).wait_recv()
+    arrived(recv2)
+    conv = convolve(short(1) * conv, spectra[1], tables)
+
+    for c in range(2):
+        for h in range(2):
+            back_v[pl.ds(2 * c + h, 32, stride=4), :] = conv[32 * h : 32 * (h + 1), 128 * c : 128 * (c + 1)]
+    for r in range(ROWS):
+        send3[r] = back_v[4 * r : 4 * r + 4, :].astype(BF16)
+    recv3[pl.ds(row, 1)] = send3[pl.ds(row, 1)]
+    row_peers(lambda r: to_row(back_trip, r).start())
 
     lane = lax.broadcasted_iota(jnp.int32, (128, 128), 1)
     sub = lax.broadcasted_iota(jnp.int32, (128, 128), 0)
@@ -420,63 +455,48 @@
     gate = sort_v[:, 384:]
     gate_v[...] = second * (gate / (1.0 + jnp.exp(-gate)))
 
-    lane = lax.broadcasted_iota(jnp.int32, (32, 128), 1)
-    sub = lax.broadcasted_iota(jnp.int32, (32, 128), 0)
-
-    def arrived(buffer):
-        for r in range(ROWS):
-            block_v[4 * r : 4 * r + 4, :] = buffer[r].astype(F32)
-
-    def short(role):
-        sides = []
-        for c in range(2):
-            here = [block_v[pl.ds(2 * c + h, 32, stride=4), :] for h in range(2)]
-            before, after = shifted(here, lane, sub)
-            weight = [own_taps[c][j, role : role + 1] for j in range(3)]
-            sides.append(
-                jnp.concatenate(
-                    [before[h] * weight[0] + here[h] * weight[1] + after[h] * weight[2] for h in range(2)], axis=0
-                )
-            )
-        return jnp.concatenate(sides, axis=1)
-
-    whole(value_trip).wait_recv()
-    arrived(recv1)
-    conv = convolve(short(0), spectra[0], tables)
-    whole(first_trip).wait_recv()
-    arrived(recv2)
-    conv = convolve(short(1) * conv, spectra[1], tables)
-
-    for c in range(2):
-        for h in range(2):
-            back_v[pl.ds(2 * c + h, 32, stride=4), :] = conv[32 * h : 32 * (h + 1), 128 * c : 128 * (c + 1)]
-    for r in range(ROWS):
-        send3[r] = back_v[4 * r : 4 * r + 4, :].astype(BF16)
-    recv3[pl.ds(row, 1)] = send3[pl.ds(row, 1)]
-    row_peers(lambda r: to_row(back_trip, r).start())
-
-    for copy in first_hops:
-        copy.wait_recv()
-    for copy in second_hops:
-        copy.start()
+    for part, side in both:
+        hopped(part, side).wait_recv()
+    for part, side in both:
+        pass_on(part, side).start()
     for part in range(2):
         for step in (1, 3):
             swap(part, step).start()
 
-    i128 = lax.broadcasted_iota(jnp.int32, (128, 256), 0)
+    p128 = lax.broadcasted_iota(jnp.int32, (128, 256), 0)
     l256 = lax.broadcasted_iota(jnp.int32, (128, 256), 1)
-    spread = jnp.where(l256 == 128 * (i128 & 1) + 64 * lax.rem(col, 2) + (i128 >> 1), 1.0, 0.0).astype(BF16)
+    spread = jnp.where((l256 >> 7 == (p128 & 1)) & ((l256 & 63) == (p128 >> 1)), 1.0, 0.0).astype(BF16)
     whole(back_trip).wait_recv()
     arrived(recv3)
     flipped = jnp.transpose(block_v[...] * gate_v[...]).astype(BF16)
-    rows = dot(flipped, spread).astype(BF16)
+    rows = dot(flipped, spread)
+    low_first = (lax.broadcasted_iota(jnp.int32, (8, 8, 128), 2) < 64) == (lax.rem(col, 2) == 0)
     for h in range(2):
-        send4[8 * h : 8 * (h + 1)] = rows[:, 128 * h : 128 * (h + 1)].reshape(8, 16, 128)
+        tiles = rows[:, 128 * h : 128 * (h + 1)].reshape(8, 2, 8, 128)
+        send4[8 * h : 8 * (h + 1)] = jnp.where(low_first, tiles[:, 0], tiles[:, 1]).astype(BF16)
     recv4[pl.ds(col, 1)] = send4[pl.ds(col, 1)]
-    col_peers(lambda c: to_col(last_trip, c).start())
-
-    for copy in second_hops:
-        copy.wait_recv()
+
+    def last(step_y, step_x):
+        c = lax.rem(y + step_y, 4) * 4 + lax.rem(x + step_x, 4)
+        return pltpu.make_async_remote_copy(
+            src_ref=send4.at[c], dst_ref=recv4.at[col], send_sem=send_sem4, recv_sem=recv_sem4.at[(4 - step_y) % 4],
+            device_id=(row, c), device_id_type=MESH,
+        )
+
+    def last_group(step_y):
+        some = recv4.at[pl.ds(0, 4 if step_y else 3)]
+        return pltpu.make_async_remote_copy(
+            src_ref=some, dst_ref=some, send_sem=send_sem4, recv_sem=recv_sem4.at[step_y],
+            device_id=(partner, col), device_id_type=MESH,
+        )
+
+    for step_y in (2, 1, 3, 0):
+        for step_x in (2, 1, 3, 0):
+            if step_y or step_x:
+                last(step_y, step_x).start()
+
+    for part, side in both:
+        pass_on(part, side).wait_recv()
     for part in range(2):
         swap(part, 2).start()
     half = w_full.at[core]
@@ -485,21 +505,38 @@
         device_id=(partner, col), device_id_type=MESH,
     )
     swapped.wait_recv()
-    whole(last_trip).wait_recv()
-    left = jnp.concatenate([recv4[2 * m] + recv4[2 * m + 1] for m in range(8)], axis=1)
-    for k in range(2):
-        for part in range(2):
-            at = 1024 * k + 512 * part
-            out_ref[0, :, at : at + 512] = dot(left, w_full[k, part].reshape(1024, 512)).astype(BF16)
+    low_lanes = lax.broadcasted_iota(jnp.int32, (8, 128), 1) < 64
+    for step_y in (0, 1, 3, 2):
+        last_group(step_y).wait_recv()
+        yy = lax.rem(y + step_y, 4)
+        lefts = []
+        for m in range(2):
+            even, odd = (recv4[4 * yy + 2 * m + e].astype(F32) for e in range(2))
+            upper_rows = jnp.where(low_lanes, even, odd)
+            lower_rows = pltpu.roll(jnp.where(low_lanes, odd, even), 64, 1)
+            lefts.append(jnp.concatenate([upper_rows, lower_rows], axis=0))
+        left = jnp.concatenate(lefts, axis=1).astype(BF16)
+        for k in range(2):
+            for part in range(2):
+                at = 1024 * k + 512 * part
+                term = dot(left, w_full[k, part, yy].reshape(256, 512))
+                if step_y:
+                    term = term + total[:, at : at + 512]
+                if step_y == 2:
+                    out_ref[0, :, at : at + 512] = term.astype(BF16)
+                else:
+                    total[:, at : at + 512] = term
 
     for trip in (value_trip, first_trip, back_trip, last_trip):
         whole(trip).wait_send()
     after_me.wait_send()
     before_me.wait_send()
     for part in range(2):
-        blocks(part).wait_send()
-    for copy in first_hops + second_hops:
-        copy.wait_send()
+        for step in (1, 2, 3):
+            spread_block(part, step).wait_send()
+    for part, side in both:
+        hopped(part, side).wait_send()
+        pass_on(part, side).wait_send()
     swapped.wait_send()
 
 
@@ -538,10 +575,11 @@
         vmem((ROWS, 4, 128), BF16), vmem((ROWS, 4, 128), BF16),
         vmem((ROWS, 4, 128), BF16), vmem((ROWS, 4, 128), BF16),
         vmem((ROWS, 4, 128), BF16), vmem((ROWS, 4, 128), BF16),
-        vmem((COLS, 16, 128), BF16), vmem((COLS, 16, 128), BF16),
+        vmem((COLS, 8, 128), BF16), vmem((COLS, 8, 128), BF16),
+        vmem((16, 2048), F32),
         sem((19,)),
-        sem, sem, sem, sem, sem, sem, sem, sem,
-        sem((2,)), sem((2,)), sem((2,)), sem((2,)), sem((2, 4)), sem((2, 4)), sem, sem,
+        sem, sem, sem, sem, sem, sem, sem, sem((4,)),
+        sem((2,)), sem((2,)), sem((2, 4)), sem((2, 4)), sem((2, 2)), sem((2, 2)), sem((2, 2)), sem((2, 2)), sem, sem,
     ]
     anywhere = pl.BlockSpec(memory_space=pltpu.HBM)
     return pl.pallas_call(
@@ -551,12 +589,15 @@
         out_specs=pl.BlockSpec(memory_space=pltpu.VMEM),
         scratch_shapes=scratch,
         compiler_params=pltpu.CompilerParams(
-            collective_id=0, has_side_effects=True, vmem_limit_bytes=67043328
+            collective_id=0, has_side_effects=True, vmem_limit_bytes=48 * 1024 * 1024
         ),
-    )(
-        tokens, w_value.T, w_first.T, w_second.T, w_gate.T, conv_taps, filter_embed, filter_freq.reshape(1, -1),
-        filter_proj, filter_decay, skip_gain, w_out, *consts,
-    )
+    )(*[
+        pltpu.with_memory_space_constraint(operand, pltpu.HBM)
+        for operand in (
+            tokens, w_value.T, w_first.T, w_second.T, w_gate.T, conv_taps, filter_embed, filter_freq.reshape(1, -1),
+            filter_proj, filter_decay, skip_gain, w_out, *consts,
+        )
+    ])
 
 
 def solution(mesh):

time: 43.4 us -> 40.6 us (0.935)
  Pallas kernels: 41.7 us -> 39.9 us
  local copies, waits for them, and re-layouts: 1.47 us -> 0.63 us
    pallas_call x1, Pallas kernels: 41.7 us -> 39.9 us  [body(): pl.pallas_call(kernel, out_shape=jax.ShapeDtypeStruct((1, 16, 2048), BF16...]
    unnamed x1, local copies, waits for them, and re-layouts: 1.47 us -> 0.63 us
where the time goes in v3:
time: 40.6 us; the launch traced here: 40.5 us
  Pallas kernels  39.9 us (98%)
  local copies, waits for them, and re-layouts  0.63 us (2%)
    pallas_call x1, Pallas kernels, body(): pl.pallas_call(kernel, out_shape=jax.ShapeDtypeStruct((1, 16, 2048), BF16...  39.9 us

profile of v3, /device:TPU:1, one launch (start us, length us, event | category | flops | bytes accessed | tf_op | source)
XLA Modules:
  0.0 40.5 jit_solution(17651181598600440853)
XLA Ops:
  0.0 39.9 %shard_map.172 = bf16[1,16,2048]{2,1,0:T(8,128)(2,1)S(1)} custom-call(bf16[1,256,2048]{2,1,0:T(8,128)(2,1)} %tokens.1, bf16[64,2048]{1,0:T(8,128)(2,1)} %bitcast.5, bf16[64,2048]{1,0:T(8,128)(2,1)} %bitcast.6, bf16[64,2048]{1,0:T(8,128)(2,1)} %bitcast.7, bf16[64,2048]{1,0:T(8,128)(2,1)} %bitcast.8, f32[3,3,64]{2,1,0:T(4,128)} %conv_taps.1, f32[33,64]{1,0:T(8,128)} %embed.1, ...), custom_call_target="tpu_custom_call" | custom-call | tf_op jit(solution)/shard_map/pallas_call | solution.py:585
  39.9 0.6 %copy.20 = bf16[1,16,2048]{2,1,0:T(8,128)(2,1)} copy(bf16[1,16,2048]{2,1,0:T(8,128)(2,1)S(1)} %shard_map.172) | data formatting | bytes 131072

commit v4 on v3

--- a/solution.py
+++ b/solution.py
@@ -152,9 +152,10 @@
     tok_v, w_v, taps_v, embed_v, freq_v, proj_v, decay_v, gain_v,
     outer_in_v, outer_out_v, twist_v, inner_in_v, inner_out_v, table_v,
     w_full, est, lag_taps, spectra, sort_v, gate_v, block_v, back_v, edge_out, edge_in,
-    send1, recv1, send2, recv2, send3, recv3, send4, recv4, total,
+    send1, recv1, send2, recv2, send3, recv3, send4, recv4, total, relay1, relay2,
     load_sem, send_sem1, recv_sem1, send_sem2, recv_sem2, send_sem3, recv_sem3, send_sem4, recv_sem4,
     edge_send, edge_recv, block_send, block_recv, hop_send, hop_recv, pass_send, pass_recv, swap_send, swap_recv,
+    relay_send, relay_recv,
 ):
     row = lax.axis_index("row")
     col = lax.axis_index("col")
@@ -175,6 +176,17 @@
         lax.fori_loop(0, 15, step, 0)
         visit(partner)
 
+    def near_peers(visit):
+        def step(i, carry):
+            away = 4 - lax.div(i, 2)
+            there = lax.rem(z + 16 + away * (1 - 2 * lax.rem(i, 2)), 16) * 2
+            visit(there)
+            visit(there + 1)
+            return carry
+
+        lax.fori_loop(0, 8, step, 0)
+        visit(partner)
+
     def col_peers(visit):
         def step(i, carry):
             visit(lax.rem(col + i, COLS))
@@ -183,7 +195,7 @@
         lax.fori_loop(1, COLS, step, 0)
 
     barrier = pltpu.get_barrier_semaphore()
-    row_peers(lambda r: pl.semaphore_signal(barrier, inc=1, device_id=(r, col), device_id_type=MESH))
+    near_peers(lambda r: pl.semaphore_signal(barrier, inc=1, device_id=(r, col), device_id_type=MESH))
     col_peers(lambda c: pl.semaphore_signal(barrier, inc=1, device_id=(row, c), device_id_type=MESH))
 
     loads = []
@@ -250,6 +262,38 @@
             device_id=(partner, col), device_id_type=MESH,
         )
 
+    def to_relay(trip, relay, i):
+        source, _, sent, _ = trip
+        held, received = relay
+        up = i < 4
+        away = 8 - i if up else 11 - i
+        sign = 1 if up else -1
+        return pltpu.make_async_remote_copy(
+            src_ref=source.at[pl.ds(lax.rem(z + 16 + sign * away, 16) * 2, 2)], dst_ref=held.at[pl.ds(2 * i, 2)],
+            send_sem=sent, recv_sem=received, device_id=(lax.rem(z + 16 + sign * 4, 16) * 2 + core, col),
+            device_id_type=MESH,
+        )
+
+    def from_relay(trip, relay, sent, i, k):
+        _, target, _, received = trip
+        up = i < 4
+        away = 4 - i if up else 7 - i
+        sign = 1 if up else -1
+        origin = lax.rem(z + 16 - sign * 4, 16) * 2 + core
+        return pltpu.make_async_remote_copy(
+            src_ref=relay[0].at[2 * i + k], dst_ref=target.at[origin], send_sem=sent, recv_sem=received,
+            device_id=(lax.rem(z + 16 + sign * away, 16) * 2 + k, col), device_id_type=MESH,
+        )
+
+    def passed(relay, sent):
+        held, received = relay
+        return pltpu.make_async_remote_copy(
+            src_ref=held, dst_ref=held, send_sem=sent, recv_sem=received,
+            device_id=(partner, col), device_id_type=MESH,
+        )
+
+    relay_order = (0, 4, 1, 5, 2, 6, 3)
+
     def edge(step, slot):
         return pltpu.make_async_remote_copy(
             src_ref=edge_out, dst_ref=edge_in.at[slot], send_sem=edge_send.at[slot], recv_sem=edge_recv.at[slot],
@@ -313,17 +357,8 @@
     first_trip = (send2, recv2, send_sem2, recv_sem2)
     back_trip = (send3, recv3, send_sem3, recv_sem3)
     last_trip = (send4, recv4, send_sem4, recv_sem4.at[0])
-
-    pl.semaphore_wait(barrier, ROWS - 1 + COLS - 1)
-    row_peers(lambda r: to_row(value_trip, r).start())
-    for step in (1, 3, 2):
-        for part in range(2):
-            spread_block(part, step).start()
-    for part, side in both:
-        hop_block(part, side, 0).start()
-    row_peers(lambda r: to_row(first_trip, r).start())
-    after_me.start()
-    before_me.start()
+    value_relay = (relay1, relay_recv.at[0])
+    first_relay = (relay2, relay_recv.at[1])
 
     for load in loads[7:]:
         load.wait()
@@ -382,7 +417,34 @@
             lag_taps[pl.ds(pl.multiple_of(to, 8), 8), :] = piece
         return carry
 
-    lax.fori_loop(0, LENGTH // 1024, lags, 0)
+    lax.fori_loop(0, LENGTH // 2048, lags, 0)
+
+    pl.semaphore_wait(barrier, 17 + COLS - 1)
+    for i in relay_order:
+        to_relay(value_trip, value_relay, i).start()
+    near_peers(lambda r: to_row(value_trip, r).start())
+    for step in (1, 3, 2):
+        for part in range(2):
+            spread_block(part, step).start()
+    for part, side in both:
+        hop_block(part, side, 0).start()
+    for i in relay_order:
+        to_relay(first_trip, first_relay, i).start()
+    near_peers(lambda r: to_row(first_trip, r).start())
+    after_me.start()
+    before_me.start()
+
+    lax.fori_loop(LENGTH // 2048, LENGTH // 1024, lags, 0)
+
+    for trip, relay, sent in (
+        (value_trip, value_relay, relay_send.at[0]),
+        (first_trip, first_relay, relay_send.at[1]),
+    ):
+        passed(relay, sent).wait_recv()
+        for i in relay_order:
+            for k in range(2):
+                from_relay(trip, relay, sent, i, k).start()
+
 
     twist = (twist_v[0], twist_v[1])
     inner_in = (inner_in_v[0], inner_in_v[1])
@@ -529,6 +591,8 @@
 
     for trip in (value_trip, first_trip, back_trip, last_trip):
         whole(trip).wait_send()
+    passed(value_relay, relay_send.at[0]).wait_send()
+    passed(first_relay, relay_send.at[1]).wait_send()
     after_me.wait_send()
     before_me.wait_send()
     for part in range(2):
@@ -577,9 +641,11 @@
         vmem((ROWS, 4, 128), BF16), vmem((ROWS, 4, 128), BF16),
         vmem((COLS, 8, 128), BF16), vmem((COLS, 8, 128), BF16),
         vmem((16, 2048), F32),
+        vmem((14, 4, 128), BF16), vmem((14, 4, 128), BF16),
         sem((19,)),
         sem, sem, sem, sem, sem, sem, sem, sem((4,)),
         sem((2,)), sem((2,)), sem((2, 4)), sem((2, 4)), sem((2, 2)), sem((2, 2)), sem((2, 2)), sem((2, 2)), sem, sem,
+        sem((2,)), sem((2,)),
     ]
     anywhere = pl.BlockSpec(memory_space=pltpu.HBM)
     return pl.pallas_call(

time: 40.6 us -> 42.4 us (1.044)
  Pallas kernels: 39.9 us -> 41.6 us
    pallas_call x1, Pallas kernels: 39.9 us -> 41.6 us  [body(): pl.pallas_call(kernel, out_shape=jax.ShapeDtypeStruct((1, 16, 2048), BF16...]
where the time goes in v4:
time: 42.4 us; the launch traced here: 42.3 us
  Pallas kernels  41.6 us (98%)
  local copies, waits for them, and re-layouts  0.63 us (1%)
    pallas_call x1, Pallas kernels, body(): pl.pallas_call(kernel, out_shape=jax.ShapeDtypeStruct((1, 16, 2048), BF16...  41.6 us

profile of v4, /device:TPU:1, one launch (start us, length us, event | category | flops | bytes accessed | tf_op | source)
XLA Modules:
  0.0 42.3 jit_solution(17586207391932399450)
XLA Ops:
  0.0 41.6 %shard_map.172 = bf16[1,16,2048]{2,1,0:T(8,128)(2,1)S(1)} custom-call(bf16[1,256,2048]{2,1,0:T(8,128)(2,1)} %tokens.1, bf16[64,2048]{1,0:T(8,128)(2,1)} %bitcast.5, bf16[64,2048]{1,0:T(8,128)(2,1)} %bitcast.6, bf16[64,2048]{1,0:T(8,128)(2,1)} %bitcast.7, bf16[64,2048]{1,0:T(8,128)(2,1)} %bitcast.8, f32[3,3,64]{2,1,0:T(4,128)} %conv_taps.1, f32[33,64]{1,0:T(8,128)} %embed.1, ...), custom_call_target="tpu_custom_call" | custom-call | tf_op jit(solution)/shard_map/pallas_call | solution.py:651
  41.6 0.6 %copy.20 = bf16[1,16,2048]{2,1,0:T(8,128)(2,1)} copy(bf16[1,16,2048]{2,1,0:T(8,128)(2,1)S(1)} %shard_map.172) | data formatting | bytes 131072

commit v5 on v4

--- a/solution.py
+++ b/solution.py
@@ -360,6 +360,21 @@
     value_relay = (relay1, relay_recv.at[0])
     first_relay = (relay2, relay_recv.at[1])
 
+    pl.semaphore_wait(barrier, 17 + COLS - 1)
+    for i in relay_order:
+        to_relay(value_trip, value_relay, i).start()
+    near_peers(lambda r: to_row(value_trip, r).start())
+    for step in (1, 3, 2):
+        for part in range(2):
+            spread_block(part, step).start()
+    for part, side in both:
+        hop_block(part, side, 0).start()
+    for i in relay_order:
+        to_relay(first_trip, first_relay, i).start()
+    near_peers(lambda r: to_row(first_trip, r).start())
+    after_me.start()
+    before_me.start()
+
     for load in loads[7:]:
         load.wait()
     scaled = embed_v[...] * freq_v[...]
@@ -417,24 +432,7 @@
             lag_taps[pl.ds(pl.multiple_of(to, 8), 8), :] = piece
         return carry
 
-    lax.fori_loop(0, LENGTH // 2048, lags, 0)
-
-    pl.semaphore_wait(barrier, 17 + COLS - 1)
-    for i in relay_order:
-        to_relay(value_trip, value_relay, i).start()
-    near_peers(lambda r: to_row(value_trip, r).start())
-    for step in (1, 3, 2):
-        for part in range(2):
-            spread_block(part, step).start()
-    for part, side in both:
-        hop_block(part, side, 0).start()
-    for i in relay_order:
-        to_relay(first_trip, first_relay, i).start()
-    near_peers(lambda r: to_row(first_trip, r).start())
-    after_me.start()
-    before_me.start()
-
-    lax.fori_loop(LENGTH // 2048, LENGTH // 1024, lags, 0)
+    lax.fori_loop(0, 6, lags, 0)
 
     for trip, relay, sent in (
         (value_trip, value_relay, relay_send.at[0]),
@@ -445,6 +443,8 @@
             for k in range(2):
                 from_relay(trip, relay, sent, i, k).start()
 
+
+    lax.fori_loop(6, 8, lags, 0)
 
     twist = (twist_v[0], twist_v[1])
     inner_in = (inner_in_v[0], inner_in_v[1])

time: 42.4 us -> 39.5 us (0.932)
  Pallas kernels: 41.6 us -> 38.7 us
    pallas_call x1, Pallas kernels: 41.6 us -> 38.7 us  [body(): pl.pallas_call(kernel, out_shape=jax.ShapeDtypeStruct((1, 16, 2048), BF16...]
where the time goes in v5:
time: 39.5 us; the launch traced here: 39.4 us
  Pallas kernels  38.7 us (98%)
  local copies, waits for them, and re-layouts  0.63 us (2%)
    pallas_call x1, Pallas kernels, body(): pl.pallas_call(kernel, out_shape=jax.ShapeDtypeStruct((1, 16, 2048), BF16...  38.7 us

profile of v5, /device:TPU:1, one launch (start us, length us, event | category | flops | bytes accessed | tf_op | source)
XLA Modules:
  0.0 39.4 jit_solution(12647079212731587094)
XLA Ops:
  0.0 38.7 %shard_map.172 = bf16[1,16,2048]{2,1,0:T(8,128)(2,1)S(1)} custom-call(bf16[1,256,2048]{2,1,0:T(8,128)(2,1)} %tokens.1, bf16[64,2048]{1,0:T(8,128)(2,1)} %bitcast.5, bf16[64,2048]{1,0:T(8,128)(2,1)} %bitcast.6, bf16[64,2048]{1,0:T(8,128)(2,1)} %bitcast.7, bf16[64,2048]{1,0:T(8,128)(2,1)} %bitcast.8, f32[3,3,64]{2,1,0:T(4,128)} %conv_taps.1, f32[33,64]{1,0:T(8,128)} %embed.1, ...), custom_call_target="tpu_custom_call" | custom-call | tf_op jit(solution)/shard_map/pallas_call | solution.py:651
  38.7 0.6 %copy.20 = bf16[1,16,2048]{2,1,0:T(8,128)(2,1)} copy(bf16[1,16,2048]{2,1,0:T(8,128)(2,1)S(1)} %shard_map.172) | data formatting | bytes 131072

commit v6 on v5

--- a/solution.py
+++ b/solution.py
@@ -364,13 +364,13 @@
     for i in relay_order:
         to_relay(value_trip, value_relay, i).start()
     near_peers(lambda r: to_row(value_trip, r).start())
+    for i in relay_order:
+        to_relay(first_trip, first_relay, i).start()
     for step in (1, 3, 2):
         for part in range(2):
             spread_block(part, step).start()
     for part, side in both:
         hop_block(part, side, 0).start()
-    for i in relay_order:
-        to_relay(first_trip, first_relay, i).start()
     near_peers(lambda r: to_row(first_trip, r).start())
     after_me.start()
     before_me.start()

time: 39.5 us -> 39.5 us (level)
  no operation moved by 1% of the time
where the time goes in v6:
time: 39.5 us; the launch traced here: 39.4 us
  Pallas kernels  38.7 us (98%)
  local copies, waits for them, and re-layouts  0.63 us (2%)
    pallas_call x1, Pallas kernels, body(): pl.pallas_call(kernel, out_shape=jax.ShapeDtypeStruct((1, 16, 2048), BF16...  38.7 us

profile of v6, /device:TPU:1, one launch (start us, length us, event | category | flops | bytes accessed | tf_op | source)
XLA Modules:
  0.0 39.4 jit_solution(8380576249366975499)
XLA Ops:
  0.0 38.7 %shard_map.172 = bf16[1,16,2048]{2,1,0:T(8,128)(2,1)S(1)} custom-call(bf16[1,256,2048]{2,1,0:T(8,128)(2,1)} %tokens.1, bf16[64,2048]{1,0:T(8,128)(2,1)} %bitcast.5, bf16[64,2048]{1,0:T(8,128)(2,1)} %bitcast.6, bf16[64,2048]{1,0:T(8,128)(2,1)} %bitcast.7, bf16[64,2048]{1,0:T(8,128)(2,1)} %bitcast.8, f32[3,3,64]{2,1,0:T(4,128)} %conv_taps.1, f32[33,64]{1,0:T(8,128)} %embed.1, ...), custom_call_target="tpu_custom_call" | custom-call | tf_op jit(solution)/shard_map/pallas_call | solution.py:651
  38.7 0.6 %copy.20 = bf16[1,16,2048]{2,1,0:T(8,128)(2,1)} copy(bf16[1,16,2048]{2,1,0:T(8,128)(2,1)S(1)} %shard_map.172) | data formatting | bytes 131072
